TPU v7x, 32 devices: a whole 2x2x4 slice. The times are simulated.
32 devices in a mesh: sp: 16 (over z, y, x), tp: 2 (over core).
Axes of the slice: x: 2, y: 2, z: 4, core: 2. Of those that a mesh axis runs over, the one named last changes fastest.
Arguments:
- tokens: bfloat16 [4096, 2048], P('sp', 'tp'), may hold values from -24 to 24
- value_weight: bfloat16 [2, 2048, 2048], P(None, 'sp', 'tp'), may hold values from -0.125 to 0.125
- outer_weight: bfloat16 [2, 2048, 2048], P(None, 'sp', 'tp'), may hold values from -0.125 to 0.125
- inner_weight: bfloat16 [2, 2048, 2048], P(None, 'sp', 'tp'), may hold values from -0.125 to 0.125
- conv_taps: float32 [2, 3, 2048], P(None, None, 'tp'), may hold values from -3.5 to 3.5
- output_weight: bfloat16 [2, 2048, 2048], P(None, 'tp', 'sp'), may hold values from -2 to 2
- norm_gain: float32 [2, 2048], P(None, 'tp'), may hold values from 0.1 to 1.9
- norm_bias: float32 [2, 2048], P(None, 'tp'), may hold values from -3 to 3
Outputs:
- mixed_out: bfloat16 [4096, 2048], P('sp', 'tp')
All inputs are finite; a program needn't handle non-finite values.
Results may differ from a plain program's by a relative error of at most 0.03.
Values may be sent and summed in bfloat16 or wider, within the bound.
A program may use at most 64 MiB of HBM per device.

v0:
```python
import jax
import jax.numpy as jnp
from jax import lax
from jax.experimental import pallas as pl
from jax.experimental.pallas import tpu as pltpu
from jax.sharding import PartitionSpec as P

LANES = 128
EPS = 1e-5


def flip(j, i):
    if i & 1:
        j = j + 1 - 2 * lax.rem(j, 2)
    if i & 2:
        j = j + 2 - 4 * lax.rem(lax.div(j, 2), 2)
    return j


def plane_size(sp, channels):
    q = 4
    while q > 1 and (sp % q or channels // q < LANES or channels % q):
        q //= 2
    return q


def make_kernel(sp, tp, q, layers, taps_count, rows, feats, depth, width, alpha):
    line = sp // q
    units = layers * 4
    model = feats * tp
    per_half = sp // tp

    def kernel(
        tok, val, outw, inn, taps, prj, gain, bias, res,
        xg, win, wout, state, ubuf, obuf, zpad, gated, part, rec1, snd2, rec2, acc, stat, stat_in, halo,
        a_send, a_recv, a_loc, u_send, u_recv, d_send, d_recv,
        g_send, g_recv, g_loc, t_send, t_recv, p_send, p_recv, r_send, r_recv, s_send, s_recv, h_send, h_recv,
    ):
        me = lax.axis_index("sp")
        c = lax.axis_index("tp")
        l = lax.div(me, q)
        j = lax.rem(me, q)

        def at_sp(other):
            return {"sp": other, "tp": c}

        def at_tp(r):
            return {"sp": me, "tp": lax.rem(c + r, tp)}

        def remote(src, dst, ssem, rsem, dev):
            return pltpu.make_async_remote_copy(
                src_ref=src, dst_ref=dst, send_sem=ssem, recv_sem=rsem,
                device_id=dev, device_id_type=pl.DeviceIdType.MESH,
            )

        def peer(i):
            return l * q + flip(j, i)

        barrier = pltpu.get_barrier_semaphore()

        def greet(dev):
            pl.semaphore_signal(barrier, inc=1, device_id=dev, device_id_type=pl.DeviceIdType.MESH)

        for i in range(1, q):
            greet(at_sp(peer(i)))
        for r in range(1, tp):
            greet(at_tp(r))

        @pl.when(l > 0)
        def _():
            greet(at_sp(me - q))

        @pl.when(l < line - 1)
        def _():
            greet(at_sp(me + q))

        neighbours = (l > 0).astype(jnp.int32) + (l < line - 1).astype(jnp.int32)
        pl.semaphore_wait(barrier, (q - 1) + (tp - 1) + neighbours)

        ORDER = (val, inn, outw, prj)

        def own_piece(k, jd):
            layer, w = divmod(k, 4)
            at = pl.ds(pl.multiple_of(jd * width, width), width)
            if w == 3:
                return prj.at[layer, at, :]
            return ORDER[w].at[layer, :, at]

        def landed(k, s):
            layer, w = divmod(k, 4)
            if w == 3:
                return wout.at[layer, s]
            return win.at[layer, w, pl.ds(pl.multiple_of(s * depth, depth), depth), :]

        def block(k, b):
            layer, w = divmod(k, 4)
            if w == 3:
                return wout.at[layer, pl.ds(b * q, q)]
            return win.at[layer, w, pl.ds(pl.multiple_of(b * (q * depth), q * depth), q * depth), :]

        def a_copy(k, i):
            return remote(own_piece(k, flip(j, i)), landed(k, me), a_send.at[k, i], a_recv.at[k, i], at_sp(peer(i)))

        def a_local(k):
            return pltpu.make_async_copy(own_piece(k, j), landed(k, me), a_loc.at[k])

        def scatter_start(k):
            a_local(k).start()
            for i in range(q - 1, 0, -1):
                a_copy(k, i).start()

        def scatter_wait(k):
            a_local(k).wait()
            for i in range(q - 1, 0, -1):
                a_copy(k, i).wait()

        def up(k, s):
            return remote(block(k, l - s), block(k, l - s), u_send.at[k, s], u_recv.at[k, s], at_sp(me + q))

        def down(k, s):
            return remote(block(k, l + s), block(k, l + s), d_send.at[k, s], d_recv.at[k, s], at_sp(me - q))

        def line_start(k, s):
            @pl.when((l - s >= 0) & (l < line - 1))
            def _():
                up(k, s).start()

            @pl.when((l + s < line) & (l > 0))
            def _():
                down(k, s).start()

        def line_recv(k, s):
            @pl.when(l - 1 - s >= 0)
            def _():
                up(k, s).wait_recv()

            @pl.when(l + 1 + s < line)
            def _():
                down(k, s).wait_recv()

        def line_sent(k, s):
            @pl.when((l - s >= 0) & (l < line - 1))
            def _():
                up(k, s).wait_send()

            @pl.when((l + s < line) & (l > 0))
            def _():
                down(k, s).wait_send()

        def src_of(layer):
            return tok if layer == 0 else state.at[layer - 1]

        def spot(layer, jj):
            return xg.at[layer, c, pl.ds(pl.multiple_of(jj * rows, rows), rows), :]

        def g_copy(layer, i):
            return remote(src_of(layer), spot(layer, j), g_send.at[layer, i], g_recv.at[layer, i], at_sp(peer(i)))

        def g_local(layer):
            return pltpu.make_async_copy(src_of(layer), spot(layer, j), g_loc.at[layer])

        def t_copy(layer, r, i):
            jj = flip(j, i)
            src = src_of(layer) if i == 0 else spot(layer, jj)
            return remote(src, spot(layer, jj), t_send.at[layer, r, i], t_recv.at[layer, r, i], at_tp(r))

        def gather_start(layer):
            g_local(layer).start()
            for i in range(q - 1, 0, -1):
                g_copy(layer, i).start()
            for r in range(1, tp):
                t_copy(layer, r, 0).start()

        def gather_forward(layer):
            for i in range(1, q):
                g_copy(layer, i).wait()
                for r in range(1, tp):
                    t_copy(layer, r, i).start()

        def gather_wait(layer):
            g_local(layer).wait()
            for i in range(q):
                for r in range(1, tp):
                    t_copy(layer, r, i).wait()

        def project(layer, w, store):
            def tile(i, carry):
                at = pl.ds(pl.multiple_of(i * rows, rows), rows)
                total = jnp.zeros((rows, width), jnp.float32)
                for cc in range(tp):
                    total = total + jnp.dot(
                        xg[layer, cc, at, :],
                        win[layer, w, pl.ds(cc * feats, feats), :],
                        preferred_element_type=jnp.float32,
                    )
                store(i, total.astype(jnp.bfloat16))
                return carry

            lax.fori_loop(0, q, tile, 0)

        def put_u(i, v):
            ubuf[pl.ds(pl.multiple_of(i * rows, rows), rows), :] = v

        def put_o(i, v):
            obuf[pl.ds(pl.multiple_of(i * rows, rows), rows), :] = v

        def put_z(i, v):
            at = pl.ds(pl.multiple_of(i * rows, rows), rows)
            zpad[pl.ds(pl.multiple_of(8 + i * rows, 8), rows), :] = v.astype(jnp.float32) * ubuf[at, :].astype(jnp.float32)

        def h_copy(layer):
            return remote(
                halo.at[layer, 0], halo.at[layer, 1], h_send.at[layer], h_recv.at[layer], at_sp(me + q)
            )

        def halo_start(layer):
            halo[layer, 0] = zpad[pl.ds(q * rows, 8), :]

            @pl.when(l < line - 1)
            def _():
                h_copy(layer).start()

        def halo_wait(layer):
            zpad[0:8, :] = jnp.zeros((8, width), jnp.float32)

            @pl.when(l > 0)
            def _():
                h_copy(layer).wait_recv()
                zpad[0:8, :] = halo[layer, 1]

            @pl.when(l < line - 1)
            def _():
                h_copy(layer).wait_send()

        def convolve(layer):
            at_c = pl.ds(pl.multiple_of(j * width, width), width)
            rates = [taps[layer, pl.ds(k, 1), at_c] for k in range(taps_count)]
            for i in range(q):
                conv = jnp.zeros((rows, width), jnp.float32)
                for k in range(taps_count):
                    first = 8 - (taps_count - 1) + k + i * rows
                    conv = conv + rates[k] * zpad[first:first + rows, :]
                at = pl.ds(i * rows, rows)
                gated[at, :] = (obuf[at, :].astype(jnp.float32) * conv).astype(jnp.bfloat16)

        def tile_at(jj):
            return pl.ds(pl.multiple_of(jj * rows, rows), rows)

        def p_copy(layer, r, i):
            at = tile_at(flip(j, i))
            return remote(
                part.at[layer, lax.rem(c + r, tp), at, :], rec1.at[layer, r - 1, at, :],
                p_send.at[layer, r, i], p_recv.at[layer, r, i], at_tp(r),
            )

        halves = 2 if q == 4 else 1
        part_rows = rows // halves

        def rows_of(h):
            return pl.ds(h * part_rows, part_rows)

        def r_copy(layer, i, h):
            at = rows_of(h)
            return remote(
                snd2.at[layer, i, at, :], rec2.at[layer, i, at, :],
                r_send.at[layer, i, h], r_recv.at[layer, i, h], at_sp(peer(i)),
            )

        def v_copy(layer, h):
            at = rows_of(h)
            return remote(
                snd2.at[layer, 3, at, :], rec2.at[layer, 3, at, :],
                r_send.at[layer, 3, h], r_recv.at[layer, 3, h], at_sp(peer(1 + h)),
            )

        def reduce_tile(layer, i):
            at = tile_at(flip(j, i))
            total = part[layer, c, at, :].astype(jnp.float32)
            for r in range(1, tp):
                p_copy(layer, r, i).wait()
                total = total + rec1[layer, r - 1, at, :].astype(jnp.float32)
            if i == 0:
                acc[...] = total
                return
            snd2[layer, i] = total.astype(jnp.bfloat16)
            if i == 3:
                for h in range(2):
                    v_copy(layer, h).start()
            elif halves == 2:
                r_copy(layer, i, i - 1).start()
            else:
                r_copy(layer, i, 0).start()

        def relay(layer):
            if halves == 2:
                for h in range(2):
                    v_copy(layer, h).wait()
                    i, at = 2 - h, rows_of(h)
                    snd2[layer, i, at, :] = (
                        snd2[layer, i, at, :].astype(jnp.float32) + rec2[layer, 3, at, :].astype(jnp.float32)
                    ).astype(jnp.bfloat16)
                    r_copy(layer, i, h).start()

        def out_product(layer):
            for i in range(q - 1, -1, -1):
                at = tile_at(flip(j, i))

                def half(n, carry):
                    cc = lax.rem(c + 1 + n, tp)
                    weight = jnp.concatenate([wout[layer, cc * per_half + b] for b in range(per_half)], axis=1)
                    part[layer, cc, at, :] = jnp.dot(
                        gated[at, :], weight, preferred_element_type=jnp.float32
                    ).astype(jnp.bfloat16)
                    return carry

                lax.fori_loop(0, tp, half, 0)
                for r in range(1, tp):
                    p_copy(layer, r, i).start()
                if i < q - 1:
                    reduce_tile(layer, i + 1)
            reduce_tile(layer, 0)
            relay(layer)

        def s_copy(layer, r):
            return remote(stat.at[layer], stat_in.at[layer, r], s_send.at[layer, r], s_recv.at[layer, r], at_tp(r))

        def finish(layer):
            pre = alpha * src_of(layer)[...].astype(jnp.float32) + acc[...]
            for i in range(1, min(q, 3)):
                for h in range(halves):
                    r_copy(layer, i, h).wait()
                pre = pre + rec2[layer, i].astype(jnp.float32)
            acc[...] = pre
            mine = jnp.sum(pre, axis=-1, keepdims=True)
            away = pre - mine * (1.0 / feats)
            spread = jnp.sum(away * away, axis=-1, keepdims=True)
            lane = lax.broadcasted_iota(jnp.int32, (rows, LANES), 1)
            stat[layer] = jnp.where(lane == 0, mine, spread)
            for r in range(1, tp):
                s_copy(layer, r).start()
            sums, spreads = [mine], [spread]
            for r in range(1, tp):
                s_copy(layer, r).wait()
                sums.append(stat_in[layer, r, :, 0:1])
                spreads.append(stat_in[layer, r, :, 1:2])
            mean = sum(sums[1:], sums[0]) * (1.0 / model)
            var = sum(spreads[1:], spreads[0])
            for s in sums:
                off = s * (1.0 / feats) - mean
                var = var + feats * off * off
            scale = lax.rsqrt(var * (1.0 / model) + EPS)
            normed = (acc[...] - mean) * scale
            y = (normed * gain[pl.ds(layer, 1), :] + bias[pl.ds(layer, 1), :]).astype(jnp.bfloat16)
            if layer == layers - 1:
                res[...] = y
            else:
                state[layer] = y

        for k in range(min(2, units)):
            scatter_start(k)
        gather_start(0)
        for k in range(2, units):
            scatter_start(k)

        def inputs_of(layer):
            gather_wait(layer)
            project(layer, 0, put_u)

        def middle_of(layer):
            project(layer, 1, put_z)
            halo_start(layer)

        def gates_of(layer):
            project(layer, 2, put_o)
            halo_wait(layer)
            convolve(layer)

        steps = line - 1
        begin = [k + k // 4 for k in range(units)]
        for t in range(begin[-1] + steps + 1):
            for k in range(units):
                if begin[k] == t:
                    scatter_wait(k)
                    line_start(k, 0)
            for k in range(units):
                s = t - begin[k]
                if 1 <= s < steps:
                    line_recv(k, s - 1)
                    line_start(k, s)
            for k in range(units):
                if t - begin[k] == steps:
                    line_recv(k, steps - 1)
            if t == begin[0] + steps - 1:
                gather_forward(0)
            if t == begin[0] + steps:
                inputs_of(0)
            if t == begin[1] + steps:
                middle_of(0)
            if t == begin[2] + steps:
                gates_of(0)
            if t == begin[3] + steps:
                out_product(0)
            if layers > 1:
                if t == begin[3] + steps + 1:
                    finish(0)
                    gather_start(1)
                if t == begin[3] + steps + 3:
                    gather_forward(1)
                if t == begin[3] + steps + 4:
                    inputs_of(1)
                    middle_of(1)
                    gates_of(1)
        if layers > 1:
            out_product(1)
            finish(1)
        for layer in range(2, layers):
            gather_start(layer)
            gather_forward(layer)
            inputs_of(layer)
            middle_of(layer)
            gates_of(layer)
            out_product(layer)
            finish(layer)
        for k in range(units):
            for s in range(steps):
                line_sent(k, s)

    return kernel


def solution(mesh):
    sp, tp = mesh.shape["sp"], mesh.shape["tp"]

    def shards(tokens, value_weight, outer_weight, inner_weight, conv_taps, output_weight, norm_gain, norm_bias):
        rows, feats = tokens.shape
        layers, depth, channels = value_weight.shape
        taps_count = conv_taps.shape[1]
        q = plane_size(sp, channels)
        width = channels // q
        line = sp // q
        model = feats * tp
        alpha = (2.0 * layers) ** 0.25
        out_cols = output_weight.shape[2]
        bf, f32 = jnp.bfloat16, jnp.float32
        kernel = make_kernel(sp, tp, q, layers, taps_count, rows, feats, depth, width, alpha)
        dma = pltpu.SemaphoreType.DMA
        units, steps = 4 * layers, max(line - 1, 1)
        others = max(tp - 1, 1)
        vm = pl.BlockSpec(memory_space=pltpu.VMEM)
        return pl.pallas_call(
            kernel,
            out_shape=jax.ShapeDtypeStruct((rows, feats), bf),
            in_specs=[vm] * 8,
            out_specs=vm,
            scratch_shapes=[
                pltpu.VMEM((layers, tp, q * rows, feats), bf),
                pltpu.VMEM((layers, 3, model, width), bf),
                pltpu.VMEM((layers, sp, width, out_cols), bf),
                pltpu.VMEM((layers, rows, feats), bf),
                pltpu.VMEM((q * rows, width), bf),
                pltpu.VMEM((q * rows, width), bf),
                pltpu.VMEM((q * rows + 8, width), f32),
                pltpu.VMEM((q * rows, width), bf),
                pltpu.VMEM((layers, tp, q * rows, feats), bf),
                pltpu.VMEM((layers, others, q * rows, feats), bf),
                pltpu.VMEM((layers, q, rows, feats), bf),
                pltpu.VMEM((layers, q, rows, feats), bf),
                pltpu.VMEM((rows, feats), f32),
                pltpu.VMEM((layers, rows, LANES), f32),
                pltpu.VMEM((layers, tp, rows, LANES), f32),
                pltpu.VMEM((layers, 2, 8, width), f32),
                dma((units, q)), dma((units, q)), dma((units,)),
                dma((units, steps)), dma((units, steps)), dma((units, steps)), dma((units, steps)),
                dma((layers, q)), dma((layers, q)), dma((layers,)),
                dma((layers, tp, q)), dma((layers, tp, q)),
                dma((layers, tp, q)), dma((layers, tp, q)),
                dma((layers, q, 2)), dma((layers, q, 2)),
                dma((layers, tp)), dma((layers, tp)),
                dma((layers,)), dma((layers,)),
            ],
            compiler_params=pltpu.CompilerParams(
                collective_id=0, has_side_effects=True, vmem_limit_bytes=60 * 1024 * 1024
            ),
        )(tokens, value_weight, outer_weight, inner_weight, conv_taps, output_weight, norm_gain, norm_bias)

    in_specs = (
        P("sp", "tp"),
        P(None, "sp", "tp"),
        P(None, "sp", "tp"),
        P(None, "sp", "tp"),
        P(None, None, "tp"),
        P(None, "tp", "sp"),
        P(None, "tp"),
        P(None, "tp"),
    )
    return jax.shard_map(shards, mesh=mesh, in_specs=in_specs, out_specs=P("sp", "tp"), check_vma=False)
```

profile of v0, /device:TPU:25, one launch (start us, length us, event | category | flops | bytes accessed | tf_op | source)
XLA Modules:
  0.0 188.4 jit_solution(10359917954718293049)
XLA Ops:
  0.0 1.4 copy.9.taps
  1.4 185.1 %shard_map.82 = bf16[256,1024]{1,0:T(8,128)(2,1)} custom-call(bf16[256,1024]{1,0:T(8,128)(2,1)} %tok.1, bf16[2,128,1024]{2,1,0:T(8,128)(2,1)} %val.1, bf16[2,128,1024]{2,1,0:T(8,128)(2,1)} %outw.1, bf16[2,128,1024]{2,1,0:T(8,128)(2,1)} %inn.1, f32[2,3,1024]{2,1,0:T(4,128)} %copy.9.taps, bf16[2,1024,128]{2,1,0:T(8,128)(2,1)} %prj.1, f32[2,1024]{1,0:T(2,128)} %gain.1, ...), custom_call_target="tpu_custom_call" | custom-call | tf_op jit(solution)/shard_map/pallas_call | solution.py:450
  186.5 1.9 copy.11
where the time goes:
time: 191 us; the launch traced here: 188 us
  Pallas kernels  185 us (97%)
  local copies, waits for them, and re-layouts  3.23 us (2%)
    pallas_call x1, Pallas kernels, shards(): pl.pallas_call(kernel, out_shape=jax.ShapeDtypeStruct((rows, feats), bf),...  185 us

commit v1 on v0

v1 whole, which is shorter than its diff:
```python
import jax
import jax.numpy as jnp
from jax import lax
from jax.experimental import pallas as pl
from jax.experimental.pallas import tpu as pltpu
from jax.sharding import PartitionSpec as P

LANES = 128
EPS = 1e-5


def flip(j, i):
    if i & 1:
        j = j + 1 - 2 * lax.rem(j, 2)
    if i & 2:
        j = j + 2 - 4 * lax.rem(lax.div(j, 2), 2)
    return j


def plane_size(sp, channels):
    q = 4
    while q > 1 and (sp % q or channels // q < LANES or channels % q):
        q //= 2
    return q


def make_kernel(sp, tp, q, layers, taps_count, rows, feats, depth, width, out_cols, alpha):
    line = sp // q
    units = layers * 4
    model = feats * tp
    per_half = sp // tp
    steps = line - 1
    halves = 2 if q == 4 else 1
    half_rows = rows // halves
    timed = line == 4 and q == 4 and tp == 2
    slots = line // tp if timed else 1
    block_cols = q * out_cols

    def kernel(
        tok, val, outw, inn, taps, prj, gain, bias, res,
        xg, win, wout, ubuf, obuf, zpad, gated, part, rec1, snd2, rec2, acc, stat, stat_in, halo,
        a_send, a_recv, a_loc, u_send, u_recv, d_send, d_recv,
        g_send, g_recv, g_loc, t_send, t_recv, p_send, p_recv, r_send, r_recv, s_send, s_recv, h_send, h_recv,
        b_send, b_recv,
    ):
        me = lax.axis_index("sp")
        c = lax.axis_index("tp")
        l = lax.div(me, q)
        j = lax.rem(me, q)

        def at_sp(other):
            return {"sp": other, "tp": c}

        def at_tp(r):
            return {"sp": me, "tp": lax.rem(c + r, tp)}

        def remote(src, dst, ssem, rsem, dev):
            return pltpu.make_async_remote_copy(
                src_ref=src, dst_ref=dst, send_sem=ssem, recv_sem=rsem,
                device_id=dev, device_id_type=pl.DeviceIdType.MESH,
            )

        def peer(i):
            return l * q + flip(j, i)

        barrier = pltpu.get_barrier_semaphore()

        def greet(dev):
            pl.semaphore_signal(barrier, inc=1, device_id=dev, device_id_type=pl.DeviceIdType.MESH)

        for i in range(1, q):
            greet(at_sp(peer(i)))
        for r in range(1, tp):
            greet(at_tp(r))

        @pl.when(l > 0)
        def _():
            greet(at_sp(me - q))

        @pl.when(l < line - 1)
        def _():
            greet(at_sp(me + q))

        neighbours = (l > 0).astype(jnp.int32) + (l < line - 1).astype(jnp.int32)
        pl.semaphore_wait(barrier, (q - 1) + (tp - 1) + neighbours)


        ORDER = (val, inn, outw, prj)

        def own_piece(k, jd):
            layer, w = divmod(k, 4)
            at = pl.ds(pl.multiple_of(jd * width, width), width)
            if w == 3:
                return prj.at[layer, at, :]
            return ORDER[w].at[layer, :, at]

        def landed(k, s):
            layer, w = divmod(k, 4)
            if w == 3:
                return wout.at[layer, s]
            return win.at[layer, w, pl.ds(pl.multiple_of(s * depth, depth), depth), :]

        def block(k, b):
            layer, w = divmod(k, 4)
            if w == 3:
                return wout.at[layer, pl.ds(b * q, q)]
            return win.at[layer, w, pl.ds(pl.multiple_of(b * (q * depth), q * depth), q * depth), :]

        def a_copy(k, i):
            return remote(own_piece(k, flip(j, i)), landed(k, me), a_send.at[k, i], a_recv.at[k, i], at_sp(peer(i)))

        def a_local(k):
            return pltpu.make_async_copy(own_piece(k, j), landed(k, me), a_loc.at[k])

        def scatter_start(k):
            a_local(k).start()
            for i in range(q - 1, 0, -1):
                a_copy(k, i).start()

        def scatter_wait(k):
            a_local(k).wait()
            for i in range(q - 1, 0, -1):
                a_copy(k, i).wait()

        def up(k, s):
            return remote(block(k, l - s), block(k, l - s), u_send.at[k, s], u_recv.at[k, s], at_sp(me + q))

        def down(k, s):
            return remote(block(k, l + s), block(k, l + s), d_send.at[k, s], d_recv.at[k, s], at_sp(me - q))

        def line_begin(k):
            scatter_wait(k)

            @pl.when(l < line - 1)
            def _():
                up(k, 0).start()

            @pl.when(l > 0)
            def _():
                down(k, 0).start()

        def line_pass(k, s):
            @pl.when((l - s >= 0) & (l < line - 1))
            def _():
                up(k, s - 1).wait_recv()
                up(k, s).start()

            @pl.when((l + s < line) & (l > 0))
            def _():
                down(k, s - 1).wait_recv()
                down(k, s).start()

        def line_end(k, s):
            @pl.when((l == line - 1) & (l - 1 - s >= 0))
            def _():
                up(k, s).wait_recv()

            @pl.when((l == 0) & (l + 1 + s < line))
            def _():
                down(k, s).wait_recv()

        def arrived(k):
            for s in range(steps):
                line_end(k, s)

        def line_sent(k, s):
            @pl.when((l - s >= 0) & (l < line - 1))
            def _():
                up(k, s).wait_send()

            @pl.when((l + s < line) & (l > 0))
            def _():
                down(k, s).wait_send()


        def part_of(h):
            return pl.ds(h * half_rows, half_rows)

        def spot(layer, jj, h):
            at = pl.ds(pl.multiple_of(jj * rows + h * half_rows, half_rows), half_rows)
            return xg.at[layer, c, at, :]

        def mine(layer, h):
            return tok.at[part_of(h)] if layer == 0 else spot(layer, j, h)

        def g_copy(layer, i, h):
            if i == 3:
                src = spot(layer, flip(j, 1 + h), h)
                return remote(src, src, g_send.at[layer, i, h], g_recv.at[layer, i, h], at_sp(peer(2 - h)))
            return remote(
                mine(layer, h), spot(layer, j, h), g_send.at[layer, i, h], g_recv.at[layer, i, h], at_sp(peer(i))
            )

        def g_local(h):
            return pltpu.make_async_copy(tok.at[part_of(h)], spot(0, j, h), g_loc.at[h])

        def t_copy(layer, r, i, h):
            src = mine(layer, h) if i == 0 else spot(layer, flip(j, i), h)
            return remote(
                src, spot(layer, flip(j, i), h), t_send.at[layer, r, i, h], t_recv.at[layer, r, i, h], at_tp(r)
            )

        def cross_start(layer, i, h):
            for r in range(1, tp):
                t_copy(layer, r, i, h).start()

        def gather_start(layer, h):
            if layer == 0:
                g_local(h).start()
            for i in range(1, min(q, 3)):
                g_copy(layer, i, h).start()
            cross_start(layer, 0, h)

        def gather_pass(layer, h):
            first = 1 + h if q == 4 else 1
            for i in range(1, min(q, 3)):
                i = first if i == 1 else 3 - first
                g_copy(layer, i, h).wait_recv()
                if q == 4 and i == first:
                    g_copy(layer, 3, h).start()
                cross_start(layer, i, h)

        def gather_last(layer, h):
            if q == 4:
                g_copy(layer, 3, h).wait_recv()
                cross_start(layer, 3, h)

        def gather_wait(layer):
            for h in range(halves):
                if layer == 0:
                    g_local(h).wait()
                for i in range(q):
                    for r in range(1, tp):
                        t_copy(layer, r, i, h).wait_recv()

        def gather_sent(layer):
            for h in range(halves):
                for i in range(1, q):
                    g_copy(layer, i, h).wait_send()
                for i in range(q):
                    for r in range(1, tp):
                        t_copy(layer, r, i, h).wait_send()

        def tile_at(jj):
            return pl.ds(pl.multiple_of(jj * rows, rows), rows)

        def project(layer, w, store):
            def tile(i, carry):
                at = tile_at(i)
                total = jnp.zeros((rows, width), jnp.float32)
                for cc in range(tp):
                    total = total + jnp.dot(
                        xg[layer, cc, at, :],
                        win[layer, w, pl.ds(cc * feats, feats), :],
                        preferred_element_type=jnp.float32,
                    )
                store(i, total.astype(jnp.bfloat16))
                return carry

            lax.fori_loop(0, q, tile, 0)

        def put_u(i, v):
            ubuf[tile_at(i), :] = v

        def put_o(i, v):
            obuf[tile_at(i), :] = v

        def put_z(i, v):
            at = tile_at(i)
            zpad[pl.ds(pl.multiple_of(8 + i * rows, 8), rows), :] = v.astype(jnp.float32) * ubuf[at, :].astype(jnp.float32)

        def h_copy(layer):
            return remote(
                halo.at[layer, 0], halo.at[layer, 1], h_send.at[layer], h_recv.at[layer], at_sp(me + q)
            )

        def halo_start(layer):
            halo[layer, 0] = zpad[pl.ds(q * rows, 8), :]

            @pl.when(l < line - 1)
            def _():
                h_copy(layer).start()

        def halo_wait(layer):
            zpad[0:8, :] = jnp.zeros((8, width), jnp.float32)

            @pl.when(l > 0)
            def _():
                h_copy(layer).wait_recv()
                zpad[0:8, :] = halo[layer, 1]

            @pl.when(l < line - 1)
            def _():
                h_copy(layer).wait_send()

        def convolve(layer):
            at_c = pl.ds(pl.multiple_of(j * width, width), width)
            rates = [taps[layer, pl.ds(k, 1), at_c] for k in range(taps_count)]
            for i in range(q):
                conv = jnp.zeros((rows, width), jnp.float32)
                for k in range(taps_count):
                    first = 8 - (taps_count - 1) + k + i * rows
                    conv = conv + rates[k] * zpad[first:first + rows, :]
                at = pl.ds(i * rows, rows)
                gated[at, :] = (obuf[at, :].astype(jnp.float32) * conv).astype(jnp.bfloat16)


        def p_copy(layer, r, i):
            at = tile_at(flip(j, i))
            return remote(
                part.at[layer, lax.rem(c + r, tp), at, :], rec1.at[layer, r - 1, at, :],
                p_send.at[layer, r, i], p_recv.at[layer, r, i], at_tp(r),
            )

        def r_copy(layer, i, h):
            at = part_of(h)
            return remote(
                snd2.at[layer, i, at, :], rec2.at[layer, i, at, :],
                r_send.at[layer, i, h], r_recv.at[layer, i, h], at_sp(peer(i)),
            )

        def v_copy(layer, h):
            at = part_of(h)
            return remote(
                snd2.at[layer, 3, at, :], rec2.at[layer, 3, at, :],
                r_send.at[layer, 3, h], r_recv.at[layer, 3, h], at_sp(peer(1 + h)),
            )

        def reduce_tile(layer, i):
            at = tile_at(flip(j, i))
            total = part[layer, c, at, :].astype(jnp.float32)
            for r in range(1, tp):
                p_copy(layer, r, i).wait()
                total = total + rec1[layer, r - 1, at, :].astype(jnp.float32)
            if i == 0:
                acc[...] = total
                return
            snd2[layer, i] = total.astype(jnp.bfloat16)
            if i == 3:
                for h in range(2):
                    v_copy(layer, h).start()
            elif halves == 1:
                r_copy(layer, i, 0).start()
            elif i == 1:
                r_copy(layer, 1, 0).start()

        def relay(layer, h):
            if halves == 2:
                v_copy(layer, h).wait()
                i, at = 2 - h, part_of(h)
                snd2[layer, i, at, :] = (
                    snd2[layer, i, at, :].astype(jnp.float32) + rec2[layer, 3, at, :].astype(jnp.float32)
                ).astype(jnp.bfloat16)
                r_copy(layer, i, h).start()
                if h == 0:
                    r_copy(layer, 2, 1).start()

        def out_product(layer):
            for i in range(q - 1, -1, -1):
                at = tile_at(flip(j, i))

                def half(n, carry):
                    cc = lax.rem(c + 1 + n, tp)
                    weight = jnp.concatenate([wout[layer, cc * per_half + b] for b in range(per_half)], axis=1)
                    part[layer, cc, at, :] = jnp.dot(
                        gated[at, :], weight, preferred_element_type=jnp.float32
                    ).astype(jnp.bfloat16)
                    return carry

                lax.fori_loop(0, tp, half, 0)
                for r in range(1, tp):
                    p_copy(layer, r, i).start()
                if i < q - 1:
                    reduce_tile(layer, i + 1)
            reduce_tile(layer, 0)


        last = layers - 1

        def nth_block(n):
            upper = (l >= line // 2).astype(jnp.int32)
            inner = ((l > 0) & (l < line - 1)).astype(jnp.int32)
            b = n
            if n < 2:
                b = n + inner * (1 - 2 * n)
            return b + upper * (line - 1 - 2 * b)

        def cols_of(m):
            return pl.ds(pl.multiple_of(m * block_cols, block_cols), block_cols)

        def q_copy(n, i):
            b = nth_block(n)
            m = lax.rem(b, slots)
            at = tile_at(flip(j, i))
            return remote(
                part.at[last, lax.div(b, slots), at, cols_of(m)], rec1.at[last, 0, at, cols_of(m)],
                p_send.at[last, m, i], p_recv.at[last, m, i], at_tp(1),
            )

        def b_copy(m, i, h):
            at = part_of(h)
            return remote(
                snd2.at[last, i, at, cols_of(m)], rec2.at[last, i, at, cols_of(m)],
                b_send.at[m, i, h], b_recv.at[m, i, h], at_sp(peer(i if i < 3 else 1 + h)),
            )

        def block_product(n):
            b = nth_block(n)
            m = lax.rem(b, slots)
            own = lax.div(b, slots) == c
            weight = jnp.concatenate([wout[last, b * q + e] for e in range(q)], axis=1)
            for i in range(q - 1, -1, -1):
                at = tile_at(flip(j, i))
                part[last, lax.div(b, slots), at, cols_of(m)] = jnp.dot(
                    gated[at, :], weight, preferred_element_type=jnp.float32
                ).astype(jnp.bfloat16)

                @pl.when(jnp.logical_not(own))
                def _():
                    q_copy(n, i).start()

            @pl.when(own)
            def _():
                for i in range(q - 1, -1, -1):
                    at = tile_at(flip(j, i))
                    q_copy(n, i).wait_recv()
                    total = part[last, c, at, cols_of(m)].astype(jnp.float32)
                    total = total + rec1[last, 0, at, cols_of(m)].astype(jnp.float32)
                    if i == 0:
                        acc[:, cols_of(m)] = total
                        continue
                    snd2[last, i, :, cols_of(m)] = total.astype(jnp.bfloat16)
                    if i == 3:
                        b_copy(m, 3, 0).start()
                        b_copy(m, 3, 1).start()
                    else:
                        b_copy(m, i, i - 1).start()

        def block_relay(n):
            b = nth_block(n)
            m = lax.rem(b, slots)

            @pl.when(lax.div(b, slots) == c)
            def _():
                for h in range(2):
                    b_copy(m, 3, h).wait_recv()
                    i, at = 2 - h, part_of(h)
                    snd2[last, i, at, cols_of(m)] = (
                        snd2[last, i, at, cols_of(m)].astype(jnp.float32)
                        + rec2[last, 3, at, cols_of(m)].astype(jnp.float32)
                    ).astype(jnp.bfloat16)
                    b_copy(m, i, h).start()

        def block_sent():
            for n in range(line):
                b = nth_block(n)

                @pl.when(lax.div(b, slots) != c)
                def _():
                    for i in range(q):
                        q_copy(n, i).wait_send()

            for m in range(slots):
                for i in range(1, 4):
                    for h in range(2):
                        b_copy(m, i, h).wait_send()

        def s_copy(layer, r, h):
            return remote(
                stat.at[layer, h], stat_in.at[layer, r, h], s_send.at[layer, r, h], s_recv.at[layer, r, h], at_tp(r)
            )

        def finish(layer, h):
            at = part_of(h)
            pre = alpha * mine(layer, h)[...].astype(jnp.float32) + acc[at, :]
            for i in range(1, min(q, 3)):
                if timed and layer == last:
                    for m in range(slots):
                        b_copy(m, i, h).wait_recv()
                else:
                    r_copy(layer, i, h).wait()
                pre = pre + rec2[layer, i, at, :].astype(jnp.float32)
            acc[at, :] = pre
            own = jnp.sum(pre, axis=-1, keepdims=True)
            away = pre - own * (1.0 / feats)
            spread = jnp.sum(away * away, axis=-1, keepdims=True)
            lane = lax.broadcasted_iota(jnp.int32, (half_rows, LANES), 1)
            stat[layer, h] = jnp.where(lane == 0, own, spread)
            for r in range(1, tp):
                s_copy(layer, r, h).start()
            sums, spreads = [own], [spread]
            for r in range(1, tp):
                s_copy(layer, r, h).wait()
                sums.append(stat_in[layer, r, h, :, 0:1])
                spreads.append(stat_in[layer, r, h, :, 1:2])
            mean = sum(sums[1:], sums[0]) * (1.0 / model)
            var = sum(spreads[1:], spreads[0])
            for s in sums:
                off = s * (1.0 / feats) - mean
                var = var + feats * off * off
            scale = lax.rsqrt(var * (1.0 / model) + EPS)
            normed = (acc[at, :] - mean) * scale
            y = (normed * gain[pl.ds(layer, 1), :] + bias[pl.ds(layer, 1), :]).astype(jnp.bfloat16)
            if layer == last:
                res[at, :] = y
            else:
                mine(layer + 1, h)[...] = y


        tasks = []

        def at_time(when, fn, *args):
            tasks.append((when, len(tasks), fn, args))

        def first_half(layer, w0, w1, w2):
            def start():
                gather_wait(layer)
                arrived(layer * 4)
                project(layer, 0, put_u)

            def middle():
                arrived(layer * 4 + 1)
                project(layer, 1, put_z)
                halo_start(layer)

            def gates():
                arrived(layer * 4 + 2)
                project(layer, 2, put_o)
                halo_wait(layer)
                convolve(layer)

            at_time(w0, start)
            at_time(w1, middle)
            at_time(w2, gates)

        def second_half(layer, when):
            def go():
                arrived(layer * 4 + 3)
                out_product(layer)

            at_time(when, go)

        if timed:
            quick, slow, piece = 11.6, 17.4, 2.9
            for k in range(4):
                at_time(0.01 * k + (0.02 if k else 0.0), scatter_start, k)
            for h in range(halves):
                at_time(0.015, gather_start, 0, h)
                at_time(8.0 + 4.0 * h, gather_pass, 0, h)
                at_time(16.0 + 4.0 * h, gather_last, 0, h)
            for k in range(4, units):
                at_time(21.0 + piece * (k - 4), scatter_start, k)
            for k in range(units):
                for s in range(1, steps):
                    at_time(3.5 + quick * k + 6.0 * s, line_pass, k, s)
                at_time(3.0 + quick * k, line_begin, k)
            reach = [3.0 + slow * (k + 1) for k in range(units)]
            for layer in range(layers):
                base = reach[4 * layer]
                if layer:
                    base = max(base, reach[4 * layer - 1] + 37.0)
                w1 = max(base + 1.0, reach[4 * layer + 1])
                w2 = max(w1 + 1.0, reach[4 * layer + 2])
                first_half(layer, base, w1, w2)
                if layer < last:
                    o = max(w2 + 2.0, reach[4 * layer + 3])
                    second_half(layer, o)
                    at_time(o + 8.0, relay, layer, 0)
                    at_time(o + 9.0, relay, layer, 1)
                    for h in range(halves):
                        f = o + 14.0 + 6.0 * h
                        at_time(f, finish, layer, h)
                        at_time(f + 0.1, gather_start, layer + 1, h)
                        at_time(f + 9.0, gather_pass, layer + 1, h)
                        at_time(f + 15.0, gather_last, layer + 1, h)
                else:
                    k = 4 * layer + 3
                    for n in range(line):
                        o = max(w2 + 2.0, reach[k] - slow + n * 6.0)
                        if n:
                            at_time(o, line_end, k, n - 1)
                        at_time(o, block_product, n)
                        at_time(o + 5.0, block_relay, n)
                    for h in range(halves):
                        at_time(reach[k] + 30.0 + h, finish, layer, h)
                    at_time(reach[k] + 33.0, block_sent)
        else:
            for k in range(units):
                at_time(-2.0 if k < 2 else -1.0, scatter_start, k)
            for h in range(halves):
                at_time(-1.5, gather_start, 0, h)
            begin = [k + k // 4 for k in range(units)]
            for k in range(units):
                at_time(begin[k], line_begin, k)
                for s in range(1, steps):
                    at_time(begin[k] + s, line_pass, k, s)
            end = begin[-1] + max(steps, 1) + 1
            ready = [begin[k] + steps for k in range(units)]
            for layer in range(layers):
                if layer == 0:
                    base = ready[0] + 0.5
                else:
                    base = max(ready[4 * layer - 1] + 4.0, end if layer > 1 else 0) + 0.5
                for h in range(halves):
                    at_time(base - 1.3, gather_pass, layer, h)
                    at_time(base - 1.2, gather_last, layer, h)
                w1 = max(base + 0.1, ready[4 * layer + 1] + 0.5)
                w2 = max(w1 + 0.1, ready[4 * layer + 2] + 0.5)
                first_half(layer, base, w1, w2)
                o = max(w2 + 0.1, ready[4 * layer + 3] + 0.5)
                second_half(layer, o)
                for h in range(2):
                    at_time(o + 0.1, relay, layer, h)
                for h in range(halves):
                    at_time(o + 0.3, finish, layer, h)
                    if layer < last:
                        at_time(o + 0.4, gather_start, layer + 1, h)

        for _, _, fn, args in sorted(tasks, key=lambda task: task[:2]):
            fn(*args)
        for layer in range(layers):
            gather_sent(layer)
        for k in range(units):
            for s in range(steps):
                line_sent(k, s)

    return kernel


def solution(mesh):
    sp, tp = mesh.shape["sp"], mesh.shape["tp"]

    def shards(tokens, value_weight, outer_weight, inner_weight, conv_taps, output_weight, norm_gain, norm_bias):
        rows, feats = tokens.shape
        layers, depth, channels = value_weight.shape
        taps_count = conv_taps.shape[1]
        q = plane_size(sp, channels)
        width = channels // q
        line = sp // q
        model = feats * tp
        alpha = (2.0 * layers) ** 0.25
        out_cols = output_weight.shape[2]
        bf, f32 = jnp.bfloat16, jnp.float32
        kernel = make_kernel(sp, tp, q, layers, taps_count, rows, feats, depth, width, out_cols, alpha)
        dma = pltpu.SemaphoreType.DMA
        units, steps = 4 * layers, max(line - 1, 1)
        others = max(tp - 1, 1)
        halves = 2 if q == 4 else 1
        half_rows = rows // halves
        vm = pl.BlockSpec(memory_space=pltpu.VMEM)
        return pl.pallas_call(
            kernel,
            out_shape=jax.ShapeDtypeStruct((rows, feats), bf),
            in_specs=[vm] * 8,
            out_specs=vm,
            scratch_shapes=[
                pltpu.VMEM((layers, tp, q * rows, feats), bf),
                pltpu.VMEM((layers, 3, model, width), bf),
                pltpu.VMEM((layers, sp, width, out_cols), bf),
                pltpu.VMEM((q * rows, width), bf),
                pltpu.VMEM((q * rows, width), bf),
                pltpu.VMEM((q * rows + 8, width), f32),
                pltpu.VMEM((q * rows, width), bf),
                pltpu.VMEM((layers, tp, q * rows, feats), bf),
                pltpu.VMEM((layers, others, q * rows, feats), bf),
                pltpu.VMEM((layers, q, rows, feats), bf),
                pltpu.VMEM((layers, q, rows, feats), bf),
                pltpu.VMEM((rows, feats), f32),
                pltpu.VMEM((layers, halves, half_rows, LANES), f32),
                pltpu.VMEM((layers, tp, halves, half_rows, LANES), f32),
                pltpu.VMEM((layers, 2, 8, width), f32),
                dma((units, q)), dma((units, q)), dma((units,)),
                dma((units, steps)), dma((units, steps)), dma((units, steps)), dma((units, steps)),
                dma((layers, q, halves)), dma((layers, q, halves)), dma((halves,)),
                dma((layers, tp, q, halves)), dma((layers, tp, q, halves)),
                dma((layers, tp, q)), dma((layers, tp, q)),
                dma((layers, q, 2)), dma((layers, q, 2)),
                dma((layers, tp, halves)), dma((layers, tp, halves)),
                dma((layers,)), dma((layers,)),
                dma((2, 4, 2)), dma((2, 4, 2)),
            ],
            compiler_params=pltpu.CompilerParams(
                collective_id=0, has_side_effects=True, vmem_limit_bytes=60 * 1024 * 1024
            ),
        )(tokens, value_weight, outer_weight, inner_weight, conv_taps, output_weight, norm_gain, norm_bias)

    in_specs = (
        P("sp", "tp"),
        P(None, "sp", "tp"),
        P(None, "sp", "tp"),
        P(None, "sp", "tp"),
        P(None, None, "tp"),
        P(None, "tp", "sp"),
        P(None, "tp"),
        P(None, "tp"),
    )
    return jax.shard_map(shards, mesh=mesh, in_specs=in_specs, out_specs=P("sp", "tp"), check_vma=False)
```

time: 191 us -> 185 us (0.969); the launches traced: 188 us -> 185 us
  Pallas kernels: 185 us -> 182 us
    pallas_call x1, Pallas kernels: 185 us -> 182 us  [shards(): pl.pallas_call(kernel, out_shape=jax.ShapeDtypeStruct((rows, feats), bf),...]
where the time goes in v1:
time: 185 us
  Pallas kernels  182 us (98%)
  local copies, waits for them, and re-layouts  3.23 us (2%)
    pallas_call x1, Pallas kernels, shards(): pl.pallas_call(kernel, out_shape=jax.ShapeDtypeStruct((rows, feats), bf),...  182 us

profile of v1, /device:TPU:25, one launch (start us, length us, event | category | flops | bytes accessed | tf_op | source)
XLA Modules:
  0.0 185.2 jit_solution(13164936567991240781)
XLA Ops:
  0.0 1.4 copy.9.taps
  1.4 181.9 %shard_map.82 = bf16[256,1024]{1,0:T(8,128)(2,1)} custom-call(bf16[256,1024]{1,0:T(8,128)(2,1)} %tok.1, bf16[2,128,1024]{2,1,0:T(8,128)(2,1)} %val.1, bf16[2,128,1024]{2,1,0:T(8,128)(2,1)} %outw.1, bf16[2,128,1024]{2,1,0:T(8,128)(2,1)} %inn.1, f32[2,3,1024]{2,1,0:T(4,128)} %copy.9.taps, bf16[2,1024,128]{2,1,0:T(8,128)(2,1)} %prj.1, f32[2,1024]{1,0:T(2,128)} %gain.1, ...), custom_call_target="tpu_custom_call" | custom-call | tf_op jit(solution)/shard_map/pallas_call | solution.py:651
  183.3 1.9 %copy.11 = bf16[256,1024]{1,0:T(8,128)(2,1)} copy(bf16[256,1024]{1,0:T(8,128)(2,1)} %shard_map.82) | data formatting | bytes 1048576

commit v2 on v1

--- a/solution.py
+++ b/solution.py
@@ -22,6 +22,10 @@
     while q > 1 and (sp % q or channels // q < LANES or channels % q):
         q //= 2
     return q
+
+
+def helped(line, q, tp, layers):
+    return line == 4 and q == 4 and tp == 2 and layers == 2
 
 
 def make_kernel(sp, tp, q, layers, taps_count, rows, feats, depth, width, out_cols, alpha):
@@ -32,7 +36,7 @@
     steps = line - 1
     halves = 2 if q == 4 else 1
     half_rows = rows // halves
-    timed = line == 4 and q == 4 and tp == 2
+    timed = helped(line, q, tp, layers)
     slots = line // tp if timed else 1
     block_cols = q * out_cols
 
@@ -41,7 +45,7 @@
         xg, win, wout, ubuf, obuf, zpad, gated, part, rec1, snd2, rec2, acc, stat, stat_in, halo,
         a_send, a_recv, a_loc, u_send, u_recv, d_send, d_recv,
         g_send, g_recv, g_loc, t_send, t_recv, p_send, p_recv, r_send, r_recv, s_send, s_recv, h_send, h_recv,
-        b_send, b_recv,
+        b_send, b_recv, n_send, n_recv, k_send, k_recv,
     ):
         me = lax.axis_index("sp")
         c = lax.axis_index("tp")
@@ -150,12 +154,72 @@
                 down(k, s - 1).wait_recv()
                 down(k, s).start()
 
+
+        def lower_inner(fn):
+            pl.when(l == 1)(fn)
+
+        def upper_inner(fn):
+            pl.when(l == 2)(fn)
+
+        def outer(fn):
+            pl.when((l == 0) | (l == 3))(fn)
+
+        def inner(fn):
+            pl.when((l == 1) | (l == 2))(fn)
+
+        def outer_begin(k):
+            @pl.when(l == 0)
+            def _():
+                scatter_wait(k)
+                up(k, 0).start()
+
+            @pl.when(l == 3)
+            def _():
+                scatter_wait(k)
+                down(k, 0).start()
+
+        def inner_ready(k):
+            @inner
+            def _():
+                scatter_wait(k)
+
+        def inward(k, s):
+            @lower_inner
+            def _():
+                if s:
+                    up(k, s - 1).wait_recv()
+                up(k, s).start()
+
+            @upper_inner
+            def _():
+                if s:
+                    down(k, s - 1).wait_recv()
+                down(k, s).start()
+
+        def outward(k, s):
+            @lower_inner
+            def _():
+                if s:
+                    down(k, s - 1).wait_recv()
+                down(k, s).start()
+
+            @upper_inner
+            def _():
+                if s:
+                    up(k, s - 1).wait_recv()
+                up(k, s).start()
+
+        def ends(k):
+            return (1, line - 2) if timed and k < 3 else (0, line - 1)
+
         def line_end(k, s):
-            @pl.when((l == line - 1) & (l - 1 - s >= 0))
+            low, high = ends(k)
+
+            @pl.when((l == high) & (l - 1 - s >= 0))
             def _():
                 up(k, s).wait_recv()
 
-            @pl.when((l == 0) & (l + 1 + s < line))
+            @pl.when((l == low) & (l + 1 + s < line))
             def _():
                 down(k, s).wait_recv()
 
@@ -164,11 +228,13 @@
                 line_end(k, s)
 
         def line_sent(k, s):
-            @pl.when((l - s >= 0) & (l < line - 1))
+            low, high = ends(k)
+
+            @pl.when((l - s >= 0) & (l < high))
             def _():
                 up(k, s).wait_send()
 
-            @pl.when((l + s < line) & (l > 0))
+            @pl.when((l + s < line) & (l > low))
             def _():
                 down(k, s).wait_send()
 
@@ -225,11 +291,11 @@
                 g_copy(layer, 3, h).wait_recv()
                 cross_start(layer, 3, h)
 
-        def gather_wait(layer):
+        def gather_wait(layer, which):
             for h in range(halves):
-                if layer == 0:
+                if layer == 0 and 0 in which:
                     g_local(h).wait()
-                for i in range(q):
+                for i in which:
                     for r in range(1, tp):
                         t_copy(layer, r, i, h).wait_recv()
 
@@ -244,30 +310,46 @@
         def tile_at(jj):
             return pl.ds(pl.multiple_of(jj * rows, rows), rows)
 
-        def project(layer, w, store):
-            def tile(i, carry):
+
+        far = layers
+        ALL, MOST, REST = (0, q), (1, q - 1), (0, 1)
+
+        def project(rows_set, layer, w, store, span):
+            first = flip(j, q - 1) if span is not ALL else 0
+
+            def tile(n, carry):
+                i = lax.rem(first + span[0] + n, q)
                 at = tile_at(i)
                 total = jnp.zeros((rows, width), jnp.float32)
                 for cc in range(tp):
                     total = total + jnp.dot(
-                        xg[layer, cc, at, :],
+                        xg[rows_set, cc, at, :],
                         win[layer, w, pl.ds(cc * feats, feats), :],
                         preferred_element_type=jnp.float32,
                     )
                 store(i, total.astype(jnp.bfloat16))
                 return carry
 
-            lax.fori_loop(0, q, tile, 0)
-
-        def put_u(i, v):
-            ubuf[tile_at(i), :] = v
-
-        def put_o(i, v):
-            obuf[tile_at(i), :] = v
-
-        def put_z(i, v):
-            at = tile_at(i)
-            zpad[pl.ds(pl.multiple_of(8 + i * rows, 8), rows), :] = v.astype(jnp.float32) * ubuf[at, :].astype(jnp.float32)
+            lax.fori_loop(0, span[1], tile, 0)
+
+        def put_u(bank):
+            def put(i, v):
+                ubuf[bank, tile_at(i), :] = v
+
+            return put
+
+        def put_o(bank):
+            def put(i, v):
+                obuf[bank, tile_at(i), :] = v
+
+            return put
+
+        def put_z(bank):
+            def put(i, v):
+                at = pl.ds(pl.multiple_of(8 + i * rows, 8), rows)
+                zpad[bank, at, :] = v.astype(jnp.float32) * ubuf[bank, tile_at(i), :].astype(jnp.float32)
+
+            return put
 
         def h_copy(layer):
             return remote(
@@ -275,34 +357,178 @@
             )
 
         def halo_start(layer):
-            halo[layer, 0] = zpad[pl.ds(q * rows, 8), :]
+            halo[layer, 0] = zpad[0, pl.ds(q * rows, 8), :]
 
             @pl.when(l < line - 1)
             def _():
                 h_copy(layer).start()
 
         def halo_wait(layer):
-            zpad[0:8, :] = jnp.zeros((8, width), jnp.float32)
+            zpad[0, 0:8, :] = jnp.zeros((8, width), jnp.float32)
 
             @pl.when(l > 0)
             def _():
                 h_copy(layer).wait_recv()
-                zpad[0:8, :] = halo[layer, 1]
+                zpad[0, 0:8, :] = halo[layer, 1]
 
             @pl.when(l < line - 1)
             def _():
                 h_copy(layer).wait_send()
 
-        def convolve(layer):
+        def convolve(layer, bank):
             at_c = pl.ds(pl.multiple_of(j * width, width), width)
-            rates = [taps[layer, pl.ds(k, 1), at_c] for k in range(taps_count)]
+            rates = [taps[k, pl.ds(layer, 1), at_c] for k in range(taps_count)]
             for i in range(q):
                 conv = jnp.zeros((rows, width), jnp.float32)
                 for k in range(taps_count):
                     first = 8 - (taps_count - 1) + k + i * rows
-                    conv = conv + rates[k] * zpad[first:first + rows, :]
+                    conv = conv + rates[k] * zpad[bank, first:first + rows, :]
                 at = pl.ds(i * rows, rows)
-                gated[at, :] = (obuf[at, :].astype(jnp.float32) * conv).astype(jnp.bfloat16)
+                gated[bank, at, :] = (obuf[bank, at, :].astype(jnp.float32) * conv).astype(jnp.bfloat16)
+
+
+        def fellow():
+            return at_sp(me + q * (1 - 2 * lax.rem(l, 2)))
+
+        def n_copy(n):
+            h = n % 2
+            src = tok.at[part_of(h)] if n < 2 else spot(far, flip(j, 1 + h), h)
+            return remote(
+                src, spot(far, j if n < 2 else flip(j, 1 + h), h), n_send.at[n], n_recv.at[n], fellow()
+            )
+
+        def e_copy(h):
+            return remote(
+                tok.at[part_of(h)], spot(far, j, h), g_send.at[far, 1 + h, h], g_recv.at[far, 1 + h, h],
+                at_sp(peer(1 + h)),
+            )
+
+        def k_copy(i):
+            at = tile_at(flip(j, i))
+            return remote(gated.at[1, at, :], gated.at[0, at, :], k_send.at[i], k_recv.at[i], fellow())
+
+        def far_send():
+            @outer
+            def _():
+                for h in range(2):
+                    e_copy(h).start()
+                for n in range(2):
+                    n_copy(n).start()
+
+        def far_pass():
+            @outer
+            def _():
+                for h in range(2):
+                    e_copy(h).wait_recv()
+                    n_copy(2 + h).start()
+
+        def far_in(h):
+            @inner
+            def _():
+                n_copy(h).wait_recv()
+                g_copy(far, 2 - h, h).start()
+                cross_start(far, 0, h)
+
+        def far_side():
+            @inner
+            def _():
+                for h in range(2):
+                    g_copy(far, 2 - h, h).wait_recv()
+                    cross_start(far, 2 - h, h)
+
+        def far_diag():
+            @inner
+            def _():
+                for h in range(2):
+                    n_copy(2 + h).wait_recv()
+                    g_copy(far, 3, h).start()
+                    cross_start(far, 1 + h, h)
+
+        def inner_gather_start(h):
+            @inner
+            def _():
+                gather_start(0, h)
+
+        def inner_pass(rows_set, h):
+            @inner
+            def _():
+                gather_pass(rows_set, h)
+
+        def inner_last(rows_set, h):
+            @inner
+            def _():
+                gather_last(rows_set, h)
+
+        def inner_project(bank, ws, span):
+            rows_set = far if bank else 0
+
+            @inner
+            def _():
+                if ws[0] == 0:
+                    gather_wait(rows_set, (3,) if span is REST else (0, 1, 2))
+                for w in ws:
+                    if bank == 0 and span is MOST:
+                        arrived(w)
+                    project(rows_set, 0, w, (put_u, put_z, put_o)[w](bank), span)
+                if bank == 0 and span is REST:
+                    @lower_inner
+                    def _():
+                        halo[0, 0] = zpad[0, pl.ds(q * rows, 8), :]
+                        h_copy(0).start()
+
+        def far_gates():
+            tail = pl.ds(q * rows, 8)
+
+            @lower_inner
+            def _():
+                zpad[1, 0:8, :] = jnp.zeros((8, width), jnp.float32)
+                zpad[0, 0:8, :] = zpad[1, tail, :]
+
+            @upper_inner
+            def _():
+                h_copy(0).wait_recv()
+                zpad[0, 0:8, :] = halo[0, 1]
+                zpad[1, 0:8, :] = zpad[0, tail, :]
+
+            @inner
+            def _():
+                convolve(0, 1)
+                k_copy(q - 1).start()
+
+        def own_gates():
+            @inner
+            def _():
+                convolve(0, 0)
+
+        def far_rest():
+            @inner
+            def _():
+                for i in range(q - 2, -1, -1):
+                    k_copy(i).start()
+
+        def far_sent():
+            @outer
+            def _():
+                for h in range(2):
+                    e_copy(h).wait_send()
+                for n in range(4):
+                    n_copy(n).wait_send()
+
+            @inner
+            def _():
+                gather_sent(0)
+                for h in range(2):
+                    g_copy(far, 2 - h, h).wait_send()
+                    g_copy(far, 3, h).wait_send()
+                    for i in range(q):
+                        for r in range(1, tp):
+                            t_copy(far, r, i, h).wait_send()
+                for i in range(q):
+                    k_copy(i).wait_send()
+
+            @lower_inner
+            def _():
+                h_copy(0).wait_send()
 
 
         def p_copy(layer, r, i):
@@ -358,12 +584,16 @@
         def out_product(layer):
             for i in range(q - 1, -1, -1):
                 at = tile_at(flip(j, i))
+                if timed and layer == 0:
+                    @outer
+                    def _():
+                        k_copy(i).wait_recv()
 
                 def half(n, carry):
                     cc = lax.rem(c + 1 + n, tp)
                     weight = jnp.concatenate([wout[layer, cc * per_half + b] for b in range(per_half)], axis=1)
                     part[layer, cc, at, :] = jnp.dot(
-                        gated[at, :], weight, preferred_element_type=jnp.float32
+                        gated[0, at, :], weight, preferred_element_type=jnp.float32
                     ).astype(jnp.bfloat16)
                     return carry
 
@@ -412,7 +642,7 @@
             for i in range(q - 1, -1, -1):
                 at = tile_at(flip(j, i))
                 part[last, lax.div(b, slots), at, cols_of(m)] = jnp.dot(
-                    gated[at, :], weight, preferred_element_type=jnp.float32
+                    gated[0, at, :], weight, preferred_element_type=jnp.float32
                 ).astype(jnp.bfloat16)
 
                 @pl.when(jnp.logical_not(own))
@@ -514,24 +744,39 @@
 
         def first_half(layer, w0, w1, w2):
             def start():
-                gather_wait(layer)
+                gather_wait(layer, range(q))
                 arrived(layer * 4)
-                project(layer, 0, put_u)
+                project(layer, layer, 0, put_u(0), ALL)
 
             def middle():
                 arrived(layer * 4 + 1)
-                project(layer, 1, put_z)
+                project(layer, layer, 1, put_z(0), ALL)
                 halo_start(layer)
 
             def gates():
                 arrived(layer * 4 + 2)
-                project(layer, 2, put_o)
+                project(layer, layer, 2, put_o(0), ALL)
                 halo_wait(layer)
-                convolve(layer)
+                convolve(layer, 0)
 
             at_time(w0, start)
             at_time(w1, middle)
             at_time(w2, gates)
+
+        def most_of(layer):
+            gather_wait(layer, (0, 1, 2))
+            for w in range(3):
+                arrived(layer * 4 + w)
+                project(layer, layer, w, (put_u, put_z, put_o)[w](0), MOST)
+
+        def rest_of(layer):
+            gather_wait(layer, (3,))
+            project(layer, layer, 0, put_u(0), REST)
+            project(layer, layer, 1, put_z(0), REST)
+            halo_start(layer)
+            project(layer, layer, 2, put_o(0), REST)
+            halo_wait(layer)
+            convolve(layer, 0)
 
         def second_half(layer, when):
             def go():
@@ -541,49 +786,67 @@
             at_time(when, go)
 
         if timed:
-            quick, slow, piece = 11.6, 17.4, 2.9
-            for k in range(4):
-                at_time(0.01 * k + (0.02 if k else 0.0), scatter_start, k)
+            at_time(-1.0, far_send)
+            for when, k in ((0.0, 0), (0.1, 1), (0.2, 3), (0.3, 4), (0.5, 2), (0.6, 5), (27.0, 6), (44.2, 7)):
+                at_time(when, scatter_start, k)
             for h in range(halves):
-                at_time(0.015, gather_start, 0, h)
-                at_time(8.0 + 4.0 * h, gather_pass, 0, h)
-                at_time(16.0 + 4.0 * h, gather_last, 0, h)
-            for k in range(4, units):
-                at_time(21.0 + piece * (k - 4), scatter_start, k)
+                at_time(0.4, inner_gather_start, h)
+                at_time((8.6, 13.6)[h], far_in, h)
+                at_time((20.0, 26.0)[h], inner_pass, 0, h)
+                at_time(43.0 + 0.1 * h, inner_last, 0, h)
+                at_time(51.0 + 0.1 * h, inner_last, far, h)
+            at_time(15.1, far_pass)
+            at_time(37.5, far_side)
+            at_time(42.5, far_diag)
+            for k, when in enumerate((3.5, 6.5, 15.0, 15.2, 15.3, 18.0, 30.0, 47.0)):
+                at_time(when, outer_begin, k)
+            for k, when in enumerate((3.5, 6.5, 27.5, 9.5, 12.5, 30.0, 44.5, 55.5)):
+                at_time(when, inner_ready, k)
+            for k, when in enumerate((3.6, 6.6, 27.6, 9.6, 49.0, 54.0, 66.0, 77.0)):
+                at_time(when, inward, k, 0)
+            for k, when in enumerate((19.0, 25.0, 31.0, 48.0, 54.1, 60.0, 71.0, 83.0)):
+                at_time(when, inward, k, 1)
+            for k, when in enumerate((9.7, 12.6, 30.1, 44.6, 55.6)):
+                at_time(when, outward, k + 3, 0)
+            for k, when in enumerate((23.5, 62.0, 73.0, 85.0, 97.0)):
+                at_time(when, outward, k + 3, 1)
+            for k, when in enumerate((54.2, 68.0, 79.0, 91.0, 103.0)):
+                at_time(when, outward, k + 3, 2)
+            at_time(33.2, inner_project, 0, (0,), MOST)
+            at_time(37.0, inner_project, 0, (1,), MOST)
+            at_time(44.7, inner_project, 0, (2,), MOST)
+            at_time(44.9, inner_project, 0, (0, 1, 2), REST)
+            at_time(45.5, inner_project, 1, (0, 1, 2), MOST)
+            at_time(53.0, inner_project, 1, (0, 1, 2), REST)
+            at_time(53.1, far_gates)
+            at_time(53.2, own_gates)
+            at_time(54.3, far_rest)
+            o = 58.0
+            second_half(0, o)
+            at_time(o + 8.0, relay, 0, 0)
+            at_time(o + 9.0, relay, 0, 1)
+            for h in range(halves):
+                f = o + 14.0 + 6.0 * h
+                at_time(f, finish, 0, h)
+                at_time(f + 0.1, gather_start, 1, h)
+                at_time(f + 9.0, gather_pass, 1, h)
+                at_time(f + 15.0, gather_last, 1, h)
+            at_time(103.5, most_of, 1)
+            at_time(106.0, rest_of, 1)
+            for n in range(line):
+                p = (110.0, 114.0, 119.0, 125.0)[n]
+                if n:
+                    at_time(p, line_end, 7, n - 1)
+                at_time(p, block_product, n)
+                at_time((126.0, 126.0, 126.5, 129.0)[n], block_relay, n)
+            at_time(127.5, far_sent)
+            at_time(128.0, gather_sent, 1)
             for k in range(units):
-                for s in range(1, steps):
-                    at_time(3.5 + quick * k + 6.0 * s, line_pass, k, s)
-                at_time(3.0 + quick * k, line_begin, k)
-            reach = [3.0 + slow * (k + 1) for k in range(units)]
-            for layer in range(layers):
-                base = reach[4 * layer]
-                if layer:
-                    base = max(base, reach[4 * layer - 1] + 37.0)
-                w1 = max(base + 1.0, reach[4 * layer + 1])
-                w2 = max(w1 + 1.0, reach[4 * layer + 2])
-                first_half(layer, base, w1, w2)
-                if layer < last:
-                    o = max(w2 + 2.0, reach[4 * layer + 3])
-                    second_half(layer, o)
-                    at_time(o + 8.0, relay, layer, 0)
-                    at_time(o + 9.0, relay, layer, 1)
-                    for h in range(halves):
-                        f = o + 14.0 + 6.0 * h
-                        at_time(f, finish, layer, h)
-                        at_time(f + 0.1, gather_start, layer + 1, h)
-                        at_time(f + 9.0, gather_pass, layer + 1, h)
-                        at_time(f + 15.0, gather_last, layer + 1, h)
-                else:
-                    k = 4 * layer + 3
-                    for n in range(line):
-                        o = max(w2 + 2.0, reach[k] - slow + n * 6.0)
-                        if n:
-                            at_time(o, line_end, k, n - 1)
-                        at_time(o, block_product, n)
-                        at_time(o + 5.0, block_relay, n)
-                    for h in range(halves):
-                        at_time(reach[k] + 30.0 + h, finish, layer, h)
-                    at_time(reach[k] + 33.0, block_sent)
+                for s in range(steps):
+                    at_time(129.5, line_sent, k, s)
+            for h in range(halves):
+                at_time(130.0 + h, finish, last, h)
+            at_time(140.0, block_sent)
         else:
             for k in range(units):
                 at_time(-2.0 if k < 2 else -1.0, scatter_start, k)
@@ -618,11 +881,12 @@
 
         for _, _, fn, args in sorted(tasks, key=lambda task: task[:2]):
             fn(*args)
-        for layer in range(layers):
-            gather_sent(layer)
-        for k in range(units):
-            for s in range(steps):
-                line_sent(k, s)
+        if not timed:
+            for layer in range(layers):
+                gather_sent(layer)
+            for k in range(units):
+                for s in range(steps):
+                    line_sent(k, s)
 
     return kernel
 
@@ -645,6 +909,8 @@
         dma = pltpu.SemaphoreType.DMA
         units, steps = 4 * layers, max(line - 1, 1)
         others = max(tp - 1, 1)
+        banks = 2 if helped(line, q, tp, layers) else 1
+        sets = layers + banks - 1
         halves = 2 if q == 4 else 1
         half_rows = rows // halves
         vm = pl.BlockSpec(memory_space=pltpu.VMEM)
@@ -654,13 +920,13 @@
             in_specs=[vm] * 8,
             out_specs=vm,
             scratch_shapes=[
-                pltpu.VMEM((layers, tp, q * rows, feats), bf),
+                pltpu.VMEM((layers + banks - 1, tp, q * rows, feats), bf),
                 pltpu.VMEM((layers, 3, model, width), bf),
                 pltpu.VMEM((layers, sp, width, out_cols), bf),
-                pltpu.VMEM((q * rows, width), bf),
-                pltpu.VMEM((q * rows, width), bf),
-                pltpu.VMEM((q * rows + 8, width), f32),
-                pltpu.VMEM((q * rows, width), bf),
+                pltpu.VMEM((banks, q * rows, width), bf),
+                pltpu.VMEM((banks, q * rows, width), bf),
+                pltpu.VMEM((banks, q * rows + 8, width), f32),
+                pltpu.VMEM((banks, q * rows, width), bf),
                 pltpu.VMEM((layers, tp, q * rows, feats), bf),
                 pltpu.VMEM((layers, others, q * rows, feats), bf),
                 pltpu.VMEM((layers, q, rows, feats), bf),
@@ -671,18 +937,18 @@
                 pltpu.VMEM((layers, 2, 8, width), f32),
                 dma((units, q)), dma((units, q)), dma((units,)),
                 dma((units, steps)), dma((units, steps)), dma((units, steps)), dma((units, steps)),
-                dma((layers, q, halves)), dma((layers, q, halves)), dma((halves,)),
-                dma((layers, tp, q, halves)), dma((layers, tp, q, halves)),
+                dma((sets, q, halves)), dma((sets, q, halves)), dma((halves,)),
+                dma((sets, tp, q, halves)), dma((sets, tp, q, halves)),
                 dma((layers, tp, q)), dma((layers, tp, q)),
                 dma((layers, q, 2)), dma((layers, q, 2)),
                 dma((layers, tp, halves)), dma((layers, tp, halves)),
                 dma((layers,)), dma((layers,)),
-                dma((2, 4, 2)), dma((2, 4, 2)),
+                dma((2, 4, 2)), dma((2, 4, 2)), dma((4,)), dma((4,)), dma((4,)), dma((4,)),
             ],
             compiler_params=pltpu.CompilerParams(
                 collective_id=0, has_side_effects=True, vmem_limit_bytes=60 * 1024 * 1024
             ),
-        )(tokens, value_weight, outer_weight, inner_weight, conv_taps, output_weight, norm_gain, norm_bias)
+        )(tokens, value_weight, outer_weight, inner_weight, jnp.swapaxes(conv_taps, 0, 1), output_weight, norm_gain, norm_bias)
 
     in_specs = (
         P("sp", "tp"),

time: 185 us -> 160 us (0.86); the launches traced: 185 us -> 158 us
  Pallas kernels: 182 us -> 156 us
    pallas_call x1, Pallas kernels: 182 us -> 156 us  [shards(): pl.pallas_call(kernel, out_shape=jax.ShapeDtypeStruct((rows, feats), bf),...]
where the time goes in v2:
time: 160 us; the launch traced here: 158 us
  Pallas kernels  156 us (98%)
  local copies, waits for them, and re-layouts  1.87 us (1%)
    pallas_call x1, Pallas kernels, shards(): pl.pallas_call(kernel, out_shape=jax.ShapeDtypeStruct((rows, feats), bf),...  156 us

profile of v2, /device:TPU:25, one launch (start us, length us, event | category | flops | bytes accessed | tf_op | source)
XLA Modules:
  0.0 158.0 jit_solution(15567825705536541566)
XLA Ops:
  0.0 156.1 %shard_map.82 = bf16[256,1024]{1,0:T(8,128)(2,1)} custom-call(bf16[256,1024]{1,0:T(8,128)(2,1)} %tok.1, bf16[2,128,1024]{2,1,0:T(8,128)(2,1)} %val.1, bf16[2,128,1024]{2,1,0:T(8,128)(2,1)} %outw.1, bf16[2,128,1024]{2,1,0:T(8,128)(2,1)} %inn.1, f32[3,2,1024]{2,1,0:T(2,128)} %bitcast.1, bf16[2,1024,128]{2,1,0:T(8,128)(2,1)} %prj.1, f32[2,1024]{1,0:T(2,128)} %gain.1, ...), custom_call_target="tpu_custom_call" | custom-call | tf_op jit(solution)/shard_map/pallas_call | solution.py:917
  156.1 1.9 %copy.10 = bf16[256,1024]{1,0:T(8,128)(2,1)} copy(bf16[256,1024]{1,0:T(8,128)(2,1)} %shard_map.82) | data formatting | bytes 1048576

commit v3 on v2

--- a/solution.py
+++ b/solution.py
@@ -46,6 +46,7 @@
         a_send, a_recv, a_loc, u_send, u_recv, d_send, d_recv,
         g_send, g_recv, g_loc, t_send, t_recv, p_send, p_recv, r_send, r_recv, s_send, s_recv, h_send, h_recv,
         b_send, b_recv, n_send, n_recv, k_send, k_recv,
+        v_send, v_recv, w_send, w_recv,
     ):
         me = lax.axis_index("sp")
         c = lax.axis_index("tp")
@@ -277,12 +278,12 @@
                 g_copy(layer, i, h).start()
             cross_start(layer, 0, h)
 
-        def gather_pass(layer, h):
+        def gather_pass(layer, h, onward=True):
             first = 1 + h if q == 4 else 1
             for i in range(1, min(q, 3)):
                 i = first if i == 1 else 3 - first
                 g_copy(layer, i, h).wait_recv()
-                if q == 4 and i == first:
+                if q == 4 and i == first and onward:
                     g_copy(layer, 3, h).start()
                 cross_start(layer, i, h)
 
@@ -371,14 +372,10 @@
                 h_copy(layer).wait_recv()
                 zpad[0, 0:8, :] = halo[layer, 1]
 
-            @pl.when(l < line - 1)
-            def _():
-                h_copy(layer).wait_send()
-
-        def convolve(layer, bank):
+        def convolve(layer, bank, tiles):
             at_c = pl.ds(pl.multiple_of(j * width, width), width)
             rates = [taps[k, pl.ds(layer, 1), at_c] for k in range(taps_count)]
-            for i in range(q):
+            for i in tiles:
                 conv = jnp.zeros((rows, width), jnp.float32)
                 for k in range(taps_count):
                     first = 8 - (taps_count - 1) + k + i * rows
@@ -452,59 +449,85 @@
         def inner_pass(rows_set, h):
             @inner
             def _():
-                gather_pass(rows_set, h)
+                gather_pass(rows_set, h, False)
+
+        def inner_onward(rows_set, h):
+            @inner
+            def _():
+                g_copy(rows_set, 3, h).start()
 
         def inner_last(rows_set, h):
             @inner
             def _():
                 gather_last(rows_set, h)
 
+        def inner_wait(rows_set, which):
+            @inner
+            def _():
+                gather_wait(rows_set, which)
+
         def inner_project(bank, ws, span):
-            rows_set = far if bank else 0
-
-            @inner
-            def _():
-                if ws[0] == 0:
-                    gather_wait(rows_set, (3,) if span is REST else (0, 1, 2))
+            @inner
+            def _():
                 for w in ws:
-                    if bank == 0 and span is MOST:
-                        arrived(w)
-                    project(rows_set, 0, w, (put_u, put_z, put_o)[w](bank), span)
-                if bank == 0 and span is REST:
-                    @lower_inner
-                    def _():
-                        halo[0, 0] = zpad[0, pl.ds(q * rows, 8), :]
-                        h_copy(0).start()
+                    project(far if bank else 0, 0, w, (put_u, put_z, put_o)[w](bank), span)
+
+        def inner_arrived(k):
+            @inner
+            def _():
+                arrived(k)
+
+        def own_edge():
+            @lower_inner
+            def _():
+                halo[0, 0] = zpad[0, pl.ds(q * rows, 8), :]
+                h_copy(0).start()
+
+        tail = pl.ds(q * rows, 8)
 
         def far_gates():
-            tail = pl.ds(q * rows, 8)
-
+            @pl.when((l == 1) | ((l == 2) & (j == 0)))
+            def _():
+                zpad[1, 0:8, :] = jnp.zeros((8, width), jnp.float32)
+
+            @pl.when((l == 2) & (j > 0))
+            def _():
+                zpad[1, 0:8, :] = zpad[0, tail, :]
+
+            @inner
+            def _():
+                convolve(0, 1, range(q))
+                k_copy(q - 1).start()
+
+        def far_first():
+            @pl.when((l == 2) & (j == 0))
+            def _():
+                zpad[1, 0:8, :] = zpad[0, tail, :]
+                convolve(0, 1, range(1))
+
+        def own_gates():
             @lower_inner
             def _():
-                zpad[1, 0:8, :] = jnp.zeros((8, width), jnp.float32)
                 zpad[0, 0:8, :] = zpad[1, tail, :]
 
             @upper_inner
             def _():
                 h_copy(0).wait_recv()
                 zpad[0, 0:8, :] = halo[0, 1]
-                zpad[1, 0:8, :] = zpad[0, tail, :]
-
-            @inner
-            def _():
-                convolve(0, 1)
-                k_copy(q - 1).start()
-
-        def own_gates():
-            @inner
-            def _():
-                convolve(0, 0)
-
-        def far_rest():
-            @inner
-            def _():
-                for i in range(q - 2, -1, -1):
+
+            @inner
+            def _():
+                convolve(0, 0, range(q))
+
+        def far_rest(*which):
+            @inner
+            def _():
+                for i in which:
                     k_copy(i).start()
+
+        def parts_sent():
+            for i in range(q):
+                p_copy(0, 1, i).wait_send()
 
         def far_sent():
             @outer
@@ -538,6 +561,12 @@
                 p_send.at[layer, r, i], p_recv.at[layer, r, i], at_tp(r),
             )
 
+
+        bit_rows = half_rows // 2
+
+        def bit_of(h, e):
+            return pl.ds(h * half_rows + e * bit_rows, bit_rows)
+
         def r_copy(layer, i, h):
             at = part_of(h)
             return remote(
@@ -545,49 +574,56 @@
                 r_send.at[layer, i, h], r_recv.at[layer, i, h], at_sp(peer(i)),
             )
 
-        def v_copy(layer, h):
-            at = part_of(h)
+        def w_copy(layer, h, e):
+            at = bit_of(h, e)
+            return remote(
+                snd2.at[layer, 2 - h, at, :], rec2.at[layer, 2 - h, at, :],
+                w_send.at[layer, h, e], w_recv.at[layer, h, e], at_sp(peer(2 - h)),
+            )
+
+        def v_copy(layer, h, e):
+            at = bit_of(h, e)
             return remote(
                 snd2.at[layer, 3, at, :], rec2.at[layer, 3, at, :],
-                r_send.at[layer, 3, h], r_recv.at[layer, 3, h], at_sp(peer(1 + h)),
+                v_send.at[layer, h, e], v_recv.at[layer, h, e], at_sp(peer(1 + h)),
             )
 
         def reduce_tile(layer, i):
             at = tile_at(flip(j, i))
             total = part[layer, c, at, :].astype(jnp.float32)
             for r in range(1, tp):
-                p_copy(layer, r, i).wait()
+                if timed:
+                    p_copy(layer, r, i).wait_recv()
+                else:
+                    p_copy(layer, r, i).wait()
                 total = total + rec1[layer, r - 1, at, :].astype(jnp.float32)
             if i == 0:
                 acc[...] = total
                 return
             snd2[layer, i] = total.astype(jnp.bfloat16)
             if i == 3:
-                for h in range(2):
-                    v_copy(layer, h).start()
+                for e in range(2):
+                    for h in range(2):
+                        v_copy(layer, h, e).start()
             elif halves == 1:
                 r_copy(layer, i, 0).start()
             elif i == 1:
                 r_copy(layer, 1, 0).start()
 
-        def relay(layer, h):
+        def relay(layer, h, e):
             if halves == 2:
-                v_copy(layer, h).wait()
-                i, at = 2 - h, part_of(h)
+                v_copy(layer, h, e).wait()
+                i, at = 2 - h, bit_of(h, e)
                 snd2[layer, i, at, :] = (
                     snd2[layer, i, at, :].astype(jnp.float32) + rec2[layer, 3, at, :].astype(jnp.float32)
                 ).astype(jnp.bfloat16)
-                r_copy(layer, i, h).start()
-                if h == 0:
+                w_copy(layer, h, e).start()
+                if h == 0 and e == 1:
                     r_copy(layer, 2, 1).start()
 
         def out_product(layer):
             for i in range(q - 1, -1, -1):
                 at = tile_at(flip(j, i))
-                if timed and layer == 0:
-                    @outer
-                    def _():
-                        k_copy(i).wait_recv()
 
                 def half(n, carry):
                     cc = lax.rem(c + 1 + n, tp)
@@ -603,6 +639,42 @@
                 if i < q - 1:
                     reduce_tile(layer, i + 1)
             reduce_tile(layer, 0)
+
+
+        def late_half():
+            return (l < line // 2).astype(jnp.int32)
+
+        def half_product(second):
+            cc = late_half() if second else 1 - late_half()
+            weight = jnp.concatenate([wout[0, cc * per_half + b] for b in range(per_half)], axis=1)
+            for i in range(q - 1, -1, -1):
+                at = tile_at(flip(j, i))
+                if not second:
+                    @outer
+                    def _():
+                        k_copy(i).wait_recv()
+
+                part[0, cc, at, :] = jnp.dot(
+                    gated[0, at, :], weight, preferred_element_type=jnp.float32
+                ).astype(jnp.bfloat16)
+
+                @pl.when(cc != c)
+                def _():
+                    p_copy(0, 1, i).start()
+
+                if i < q - 1:
+                    @pl.when(cc == c)
+                    def _():
+                        reduce_tile(0, i + 1)
+
+            @pl.when(cc == c)
+            def _():
+                reduce_tile(0, 0)
+
+        def half_relay(second, h, e):
+            @pl.when((late_half() == c) if second else (late_half() != c))
+            def _():
+                relay(0, h, e)
 
 
         last = layers - 1
@@ -663,8 +735,8 @@
                     if i == 3:
                         b_copy(m, 3, 0).start()
                         b_copy(m, 3, 1).start()
-                    else:
-                        b_copy(m, i, i - 1).start()
+                    elif i == 1:
+                        b_copy(m, 1, 0).start()
 
         def block_relay(n):
             b = nth_block(n)
@@ -680,6 +752,8 @@
                         + rec2[last, 3, at, cols_of(m)].astype(jnp.float32)
                     ).astype(jnp.bfloat16)
                     b_copy(m, i, h).start()
+                    if h == 0:
+                        b_copy(m, 2, 1).start()
 
         def block_sent():
             for n in range(line):
@@ -707,6 +781,9 @@
                 if timed and layer == last:
                     for m in range(slots):
                         b_copy(m, i, h).wait_recv()
+                elif halves == 2 and i == 2 - h:
+                    for e in range(2):
+                        w_copy(layer, h, e).wait()
                 else:
                     r_copy(layer, i, h).wait()
                 pre = pre + rec2[layer, i, at, :].astype(jnp.float32)
@@ -757,15 +834,15 @@
                 arrived(layer * 4 + 2)
                 project(layer, layer, 2, put_o(0), ALL)
                 halo_wait(layer)
-                convolve(layer, 0)
+                convolve(layer, 0, range(q))
+                halo_sent(layer)
 
             at_time(w0, start)
             at_time(w1, middle)
             at_time(w2, gates)
 
-        def most_of(layer):
-            gather_wait(layer, (0, 1, 2))
-            for w in range(3):
+        def most_of(layer, ws):
+            for w in ws:
                 arrived(layer * 4 + w)
                 project(layer, layer, w, (put_u, put_z, put_o)[w](0), MOST)
 
@@ -774,9 +851,16 @@
             project(layer, layer, 0, put_u(0), REST)
             project(layer, layer, 1, put_z(0), REST)
             halo_start(layer)
+
+        def gates_of(layer):
             project(layer, layer, 2, put_o(0), REST)
             halo_wait(layer)
-            convolve(layer, 0)
+            convolve(layer, 0, range(q))
+
+        def halo_sent(layer):
+            @pl.when(l < line - 1)
+            def _():
+                h_copy(layer).wait_send()
 
         def second_half(layer, when):
             def go():
@@ -787,52 +871,78 @@
 
         if timed:
             at_time(-1.0, far_send)
-            for when, k in ((0.0, 0), (0.1, 1), (0.2, 3), (0.3, 4), (0.5, 2), (0.6, 5), (27.0, 6), (44.2, 7)):
+            for when, k in ((0.0, 0), (0.1, 1), (0.2, 3), (0.3, 4), (0.5, 2), (0.6, 5), (13.7, 6), (13.8, 7)):
                 at_time(when, scatter_start, k)
             for h in range(halves):
                 at_time(0.4, inner_gather_start, h)
                 at_time((8.6, 13.6)[h], far_in, h)
                 at_time((20.0, 26.0)[h], inner_pass, 0, h)
-                at_time(43.0 + 0.1 * h, inner_last, 0, h)
-                at_time(51.0 + 0.1 * h, inner_last, far, h)
+                at_time(42.55 + 0.01 * h, inner_onward, 0, h)
+                at_time(53.19 + 0.001 * h, inner_last, 0, h)
+                at_time(51.0 + 0.05 * h, inner_last, far, h)
             at_time(15.1, far_pass)
             at_time(37.5, far_side)
             at_time(42.5, far_diag)
-            for k, when in enumerate((3.5, 6.5, 15.0, 15.2, 15.3, 18.0, 30.0, 47.0)):
+            for k, when in enumerate((3.5, 6.5, 15.0, 15.2, 15.3, 18.0, 22.0, 24.0)):
                 at_time(when, outer_begin, k)
-            for k, when in enumerate((3.5, 6.5, 27.5, 9.5, 12.5, 30.0, 44.5, 55.5)):
+            for k, when in enumerate((3.5, 6.5, 27.5, 9.5, 12.5, 30.0, 42.6, 42.7)):
                 at_time(when, inner_ready, k)
-            for k, when in enumerate((3.6, 6.6, 27.6, 9.6, 49.0, 54.0, 66.0, 77.0)):
+            for k, when in enumerate((3.6, 6.6, 27.6, 9.6, 54.22, 55.25, 66.0, 77.0)):
                 at_time(when, inward, k, 0)
-            for k, when in enumerate((19.0, 25.0, 31.0, 48.0, 54.1, 60.0, 71.0, 83.0)):
+            for k, when in enumerate((19.0, 25.0, 31.0, 51.5, 55.1, 60.0, 71.0, 83.0)):
                 at_time(when, inward, k, 1)
-            for k, when in enumerate((9.7, 12.6, 30.1, 44.6, 55.6)):
+            for k, when in enumerate((9.7, 12.6, 30.1, 42.61, 42.71)):
                 at_time(when, outward, k + 3, 0)
             for k, when in enumerate((23.5, 62.0, 73.0, 85.0, 97.0)):
                 at_time(when, outward, k + 3, 1)
-            for k, when in enumerate((54.2, 68.0, 79.0, 91.0, 103.0)):
+            for k, when in enumerate((54.2, 68.0, 79.0, 91.0)):
                 at_time(when, outward, k + 3, 2)
+            at_time(33.1, inner_wait, 0, (0, 1, 2))
+            at_time(33.1, inner_arrived, 0)
             at_time(33.2, inner_project, 0, (0,), MOST)
+            at_time(37.0, inner_arrived, 1)
             at_time(37.0, inner_project, 0, (1,), MOST)
-            at_time(44.7, inner_project, 0, (2,), MOST)
-            at_time(44.9, inner_project, 0, (0, 1, 2), REST)
-            at_time(45.5, inner_project, 1, (0, 1, 2), MOST)
-            at_time(53.0, inner_project, 1, (0, 1, 2), REST)
+            at_time(43.5, inner_wait, far, (0, 1, 2))
+            at_time(43.6, inner_project, 1, (0, 1), MOST)
+            at_time(45.5, inner_arrived, 2)
+            at_time(45.6, inner_project, 1, (2,), MOST)
+            at_time(52.0, inner_wait, far, (3,))
+            at_time(52.1, inner_project, 1, (0, 1, 2), REST)
             at_time(53.1, far_gates)
-            at_time(53.2, own_gates)
-            at_time(54.3, far_rest)
+            at_time(53.15, far_rest, 2, 1)
+            at_time(53.18, inner_project, 0, (2,), MOST)
+            at_time(53.2, inner_wait, 0, (3,))
+            at_time(53.21, inner_project, 0, (0, 1), REST)
+            at_time(53.22, own_edge)
+            at_time(53.23, far_first)
+            at_time(53.24, far_rest, 0)
+            at_time(54.21, inner_project, 0, (2,), REST)
+            at_time(55.3, own_gates)
             o = 58.0
-            second_half(0, o)
-            at_time(o + 8.0, relay, 0, 0)
-            at_time(o + 9.0, relay, 0, 1)
+            at_time(o, line_end, 3, 0)
+            at_time(o, half_product, False)
+            for e in range(2):
+                for h in range(2):
+                    at_time(o + 4.0 + 0.1 * e + 0.01 * h, half_relay, False, h, e)
+            at_time(o + 4.2, line_end, 3, 1)
+            at_time(o + 4.2, line_end, 3, 2)
+            at_time(o + 4.3, half_product, True)
+            for e in range(2):
+                for h in range(2):
+                    at_time(o + 9.0 + 0.1 * e + 0.01 * h, half_relay, True, h, e)
             for h in range(halves):
                 f = o + 14.0 + 6.0 * h
                 at_time(f, finish, 0, h)
                 at_time(f + 0.1, gather_start, 1, h)
                 at_time(f + 9.0, gather_pass, 1, h)
-                at_time(f + 15.0, gather_last, 1, h)
-            at_time(103.5, most_of, 1)
-            at_time(106.0, rest_of, 1)
+                at_time(93.0 + 0.1 * h, gather_last, 1, h)
+            at_time(88.0, gather_wait, 1, (0, 1, 2))
+            at_time(88.1, most_of, 1, (0, 1))
+            at_time(92.0, most_of, 1, (2,))
+            at_time(94.0, rest_of, 1)
+            at_time(103.0, outward, units - 1, 2)
+            at_time(106.2, gates_of, 1)
+            at_time(128.0, halo_sent, 1)
             for n in range(line):
                 p = (110.0, 114.0, 119.0, 125.0)[n]
                 if n:
@@ -840,6 +950,7 @@
                 at_time(p, block_product, n)
                 at_time((126.0, 126.0, 126.5, 129.0)[n], block_relay, n)
             at_time(127.5, far_sent)
+            at_time(127.6, parts_sent)
             at_time(128.0, gather_sent, 1)
             for k in range(units):
                 for s in range(steps):
@@ -872,8 +983,9 @@
                 first_half(layer, base, w1, w2)
                 o = max(w2 + 0.1, ready[4 * layer + 3] + 0.5)
                 second_half(layer, o)
-                for h in range(2):
-                    at_time(o + 0.1, relay, layer, h)
+                for e in range(2):
+                    for h in range(2):
+                        at_time(o + 0.1, relay, layer, h, e)
                 for h in range(halves):
                     at_time(o + 0.3, finish, layer, h)
                     if layer < last:
@@ -944,6 +1056,7 @@
                 dma((layers, tp, halves)), dma((layers, tp, halves)),
                 dma((layers,)), dma((layers,)),
                 dma((2, 4, 2)), dma((2, 4, 2)), dma((4,)), dma((4,)), dma((4,)), dma((4,)),
+                dma((layers, 2, 2)), dma((layers, 2, 2)), dma((layers, 2, 2)), dma((layers, 2, 2)),
             ],
             compiler_params=pltpu.CompilerParams(
                 collective_id=0, has_side_effects=True, vmem_limit_bytes=60 * 1024 * 1024

time: 160 us -> 147 us (0.919)
  Pallas kernels: 156 us -> 143 us
    pallas_call x1, Pallas kernels: 156 us -> 143 us  [shards(): pl.pallas_call(kernel, out_shape=jax.ShapeDtypeStruct((rows, feats), bf),...]
where the time goes in v3:
time: 147 us; the launch traced here: 145 us
  Pallas kernels  143 us (97%)
  local copies, waits for them, and re-layouts  1.87 us (1%)
    pallas_call x1, Pallas kernels, shards(): pl.pallas_call(kernel, out_shape=jax.ShapeDtypeStruct((rows, feats), bf),...  143 us

profile of v3, /device:TPU:25, one launch (start us, length us, event | category | flops | bytes accessed | tf_op | source)
XLA Modules:
  0.0 144.5 jit_solution(3315881164684239274)
XLA Ops:
  0.0 142.6 %shard_map.82 = bf16[256,1024]{1,0:T(8,128)(2,1)} custom-call(bf16[256,1024]{1,0:T(8,128)(2,1)} %tok.1, bf16[2,128,1024]{2,1,0:T(8,128)(2,1)} %val.1, bf16[2,128,1024]{2,1,0:T(8,128)(2,1)} %outw.1, bf16[2,128,1024]{2,1,0:T(8,128)(2,1)} %inn.1, f32[3,2,1024]{2,1,0:T(2,128)} %bitcast.1, bf16[2,1024,128]{2,1,0:T(8,128)(2,1)} %prj.1, f32[2,1024]{1,0:T(2,128)} %gain.1, ...), custom_call_target="tpu_custom_call" | custom-call | tf_op jit(solution)/shard_map/pallas_call | solution.py:1029
  142.6 1.9 %copy.10 = bf16[256,1024]{1,0:T(8,128)(2,1)} copy(bf16[256,1024]{1,0:T(8,128)(2,1)} %shard_map.82) | data formatting | bytes 1048576

commit v4 on v3

--- a/solution.py
+++ b/solution.py
@@ -43,10 +43,10 @@
     def kernel(
         tok, val, outw, inn, taps, prj, gain, bias, res,
         xg, win, wout, ubuf, obuf, zpad, gated, part, rec1, snd2, rec2, acc, stat, stat_in, halo,
-        a_send, a_recv, a_loc, u_send, u_recv, d_send, d_recv,
+        a_send, a_recv, u_send, u_recv, d_send, d_recv,
         g_send, g_recv, g_loc, t_send, t_recv, p_send, p_recv, r_send, r_recv, s_send, s_recv, h_send, h_recv,
         b_send, b_recv, n_send, n_recv, k_send, k_recv,
-        v_send, v_recv, w_send, w_recv,
+        v_recv, w_recv, e_recv,
     ):
         me = lax.axis_index("sp")
         c = lax.axis_index("tp")
@@ -112,26 +112,36 @@
             return win.at[layer, w, pl.ds(pl.multiple_of(b * (q * depth), q * depth), q * depth), :]
 
         def a_copy(k, i):
-            return remote(own_piece(k, flip(j, i)), landed(k, me), a_send.at[k, i], a_recv.at[k, i], at_sp(peer(i)))
+            return remote(own_piece(k, flip(j, i)), landed(k, me), a_send.at[k], a_recv.at[k], at_sp(peer(i)))
 
         def a_local(k):
-            return pltpu.make_async_copy(own_piece(k, j), landed(k, me), a_loc.at[k])
+            return pltpu.make_async_copy(own_piece(k, j), landed(k, me), a_recv.at[k])
 
         def scatter_start(k):
             a_local(k).start()
             for i in range(q - 1, 0, -1):
                 a_copy(k, i).start()
 
+
+        def take(ref, sem):
+            pltpu.make_async_copy(ref, ref, sem).wait()
+
         def scatter_wait(k):
-            a_local(k).wait()
-            for i in range(q - 1, 0, -1):
-                a_copy(k, i).wait()
+            take(block(k, l), a_recv.at[k])
+
+        def scatter_sent(k):
+            layer, w = divmod(k, 4)
+            if q > 1:
+                n = q - 1
+                take(wout.at[layer, pl.ds(0, n)] if w == 3 else win.at[layer, w, pl.ds(0, n * depth), :], a_send.at[k])
 
         def up(k, s):
-            return remote(block(k, l - s), block(k, l - s), u_send.at[k, s], u_recv.at[k, s], at_sp(me + q))
+            sems = (u_send.at[k], u_recv.at[k, s]) if timed else (u_send.at[k, s], u_recv.at[k, s])
+            return remote(block(k, l - s), block(k, l - s), *sems, at_sp(me + q))
 
         def down(k, s):
-            return remote(block(k, l + s), block(k, l + s), d_send.at[k, s], d_recv.at[k, s], at_sp(me - q))
+            sems = (u_send.at[k], u_recv.at[k, steps - 1 - s]) if timed else (d_send.at[k, s], d_recv.at[k, s])
+            return remote(block(k, l + s), block(k, l + s), *sems, at_sp(me - q))
 
         def line_begin(k):
             scatter_wait(k)
@@ -229,15 +239,25 @@
                 line_end(k, s)
 
         def line_sent(k, s):
-            low, high = ends(k)
-
-            @pl.when((l - s >= 0) & (l < high))
+            @pl.when((l - s >= 0) & (l < line - 1))
             def _():
                 up(k, s).wait_send()
 
-            @pl.when((l + s < line) & (l > low))
+            @pl.when((l + s < line) & (l > 0))
             def _():
                 down(k, s).wait_send()
+
+        def all_sent(k):
+            each = q * depth * width // feats
+            scatter_sent(k)
+
+            @outer
+            def _():
+                take(xg.at[0, 0, pl.ds(0, each), :], u_send.at[k])
+
+            @inner
+            def _():
+                take(xg.at[0, 0, pl.ds(0, (2 if k < 3 else 5) * each), :], u_send.at[k])
 
 
         def part_of(h):
@@ -253,18 +273,27 @@
         def g_copy(layer, i, h):
             if i == 3:
                 src = spot(layer, flip(j, 1 + h), h)
-                return remote(src, src, g_send.at[layer, i, h], g_recv.at[layer, i, h], at_sp(peer(2 - h)))
-            return remote(
-                mine(layer, h), spot(layer, j, h), g_send.at[layer, i, h], g_recv.at[layer, i, h], at_sp(peer(i))
-            )
+                return remote(src, src, g_send.at[layer], g_recv.at[layer, i - 1, h], at_sp(peer(2 - h)))
+            return remote(
+                mine(layer, h), spot(layer, j, h), g_send.at[layer], g_recv.at[layer, i - 1, h], at_sp(peer(i))
+            )
+
+        def g_piece(i, e):
+            first = (j if i == 2 else flip(j, 2)) * rows + half_rows + e * (half_rows // 2)
+            src = xg.at[1, c, pl.ds(pl.multiple_of(first, half_rows // 2), half_rows // 2), :]
+            got = e_recv.at[e] if i == 2 else g_recv.at[1, 2, 1]
+            return remote(src, src, g_send.at[1], got, at_sp(peer(2 if i == 2 else 1)))
 
         def g_local(h):
-            return pltpu.make_async_copy(tok.at[part_of(h)], spot(0, j, h), g_loc.at[h])
+            return pltpu.make_async_copy(tok.at[part_of(h)], spot(0, j, h), g_loc.at[0])
+
+        def rows_like(n):
+            return xg.at[0, 0, pl.ds(0, n * rows), :]
 
         def t_copy(layer, r, i, h):
             src = mine(layer, h) if i == 0 else spot(layer, flip(j, i), h)
             return remote(
-                src, spot(layer, flip(j, i), h), t_send.at[layer, r, i, h], t_recv.at[layer, r, i, h], at_tp(r)
+                src, spot(layer, flip(j, i), h), t_send.at[layer, r - 1], t_recv.at[layer, r - 1, i // 3], at_tp(r)
             )
 
         def cross_start(layer, i, h):
@@ -275,16 +304,25 @@
             if layer == 0:
                 g_local(h).start()
             for i in range(1, min(q, 3)):
-                g_copy(layer, i, h).start()
+                if timed and layer == 1 and i == 2 and h == 1:
+                    for e in range(2):
+                        g_piece(2, e).start()
+                else:
+                    g_copy(layer, i, h).start()
             cross_start(layer, 0, h)
 
         def gather_pass(layer, h, onward=True):
             first = 1 + h if q == 4 else 1
             for i in range(1, min(q, 3)):
                 i = first if i == 1 else 3 - first
-                g_copy(layer, i, h).wait_recv()
-                if q == 4 and i == first and onward:
-                    g_copy(layer, 3, h).start()
+                if timed and layer == 1 and i == 2 and h == 1:
+                    for e in range(2):
+                        g_piece(2, e).wait_recv()
+                        g_piece(3, e).start()
+                else:
+                    g_copy(layer, i, h).wait_recv()
+                    if q == 4 and i == first and onward:
+                        g_copy(layer, 3, h).start()
                 cross_start(layer, i, h)
 
         def gather_last(layer, h):
@@ -292,21 +330,17 @@
                 g_copy(layer, 3, h).wait_recv()
                 cross_start(layer, 3, h)
 
-        def gather_wait(layer, which):
-            for h in range(halves):
-                if layer == 0 and 0 in which:
-                    g_local(h).wait()
-                for i in which:
-                    for r in range(1, tp):
-                        t_copy(layer, r, i, h).wait_recv()
+        def gather_wait(layer, rest):
+            for r in range(1, tp):
+                take(rows_like(1 if rest else min(q, 3)), t_recv.at[layer, r - 1, 1 if rest else 0])
+            if layer == 0 and not rest:
+                take(rows_like(1), g_loc.at[0])
 
         def gather_sent(layer):
-            for h in range(halves):
-                for i in range(1, q):
-                    g_copy(layer, i, h).wait_send()
-                for i in range(q):
-                    for r in range(1, tp):
-                        t_copy(layer, r, i, h).wait_send()
+            if q > 1:
+                take(rows_like(q - 1), g_send.at[layer])
+            for r in range(1, tp):
+                take(rows_like(q), t_send.at[layer, r - 1])
 
         def tile_at(jj):
             return pl.ds(pl.multiple_of(jj * rows, rows), rows)
@@ -391,18 +425,18 @@
             h = n % 2
             src = tok.at[part_of(h)] if n < 2 else spot(far, flip(j, 1 + h), h)
             return remote(
-                src, spot(far, j if n < 2 else flip(j, 1 + h), h), n_send.at[n], n_recv.at[n], fellow()
+                src, spot(far, j if n < 2 else flip(j, 1 + h), h), n_send.at[0], n_recv.at[n], fellow()
             )
 
         def e_copy(h):
             return remote(
-                tok.at[part_of(h)], spot(far, j, h), g_send.at[far, 1 + h, h], g_recv.at[far, 1 + h, h],
+                tok.at[part_of(h)], spot(far, j, h), g_send.at[far], g_recv.at[far, h, h],
                 at_sp(peer(1 + h)),
             )
 
         def k_copy(i):
             at = tile_at(flip(j, i))
-            return remote(gated.at[1, at, :], gated.at[0, at, :], k_send.at[i], k_recv.at[i], fellow())
+            return remote(gated.at[1, at, :], gated.at[0, at, :], k_send.at[0], k_recv.at[i], fellow())
 
         def far_send():
             @outer
@@ -461,10 +495,10 @@
             def _():
                 gather_last(rows_set, h)
 
-        def inner_wait(rows_set, which):
-            @inner
-            def _():
-                gather_wait(rows_set, which)
+        def inner_wait(rows_set, rest):
+            @inner
+            def _():
+                gather_wait(rows_set, rest)
 
         def inner_project(bank, ws, span):
             @inner
@@ -525,29 +559,19 @@
                 for i in which:
                     k_copy(i).start()
 
-        def parts_sent():
-            for i in range(q):
-                p_copy(0, 1, i).wait_send()
-
         def far_sent():
             @outer
             def _():
-                for h in range(2):
-                    e_copy(h).wait_send()
-                for n in range(4):
-                    n_copy(n).wait_send()
+                take(rows_like(1), g_send.at[far])
+                take(rows_like(2), n_send.at[0])
 
             @inner
             def _():
                 gather_sent(0)
-                for h in range(2):
-                    g_copy(far, 2 - h, h).wait_send()
-                    g_copy(far, 3, h).wait_send()
-                    for i in range(q):
-                        for r in range(1, tp):
-                            t_copy(far, r, i, h).wait_send()
-                for i in range(q):
-                    k_copy(i).wait_send()
+                take(rows_like(2), g_send.at[far])
+                for r in range(1, tp):
+                    take(rows_like(q), t_send.at[far, r - 1])
+                take(gated.at[1], k_send.at[0])
 
             @lower_inner
             def _():
@@ -558,7 +582,7 @@
             at = tile_at(flip(j, i))
             return remote(
                 part.at[layer, lax.rem(c + r, tp), at, :], rec1.at[layer, r - 1, at, :],
-                p_send.at[layer, r, i], p_recv.at[layer, r, i], at_tp(r),
+                p_send.at[layer, r - 1], p_recv.at[layer, r - 1, i], at_tp(r),
             )
 
 
@@ -571,31 +595,28 @@
             at = part_of(h)
             return remote(
                 snd2.at[layer, i, at, :], rec2.at[layer, i, at, :],
-                r_send.at[layer, i, h], r_recv.at[layer, i, h], at_sp(peer(i)),
+                r_send.at[layer], r_recv.at[layer, i - 1], at_sp(peer(i)),
             )
 
         def w_copy(layer, h, e):
             at = bit_of(h, e)
             return remote(
                 snd2.at[layer, 2 - h, at, :], rec2.at[layer, 2 - h, at, :],
-                w_send.at[layer, h, e], w_recv.at[layer, h, e], at_sp(peer(2 - h)),
+                r_send.at[layer], w_recv.at[layer, h, e], at_sp(peer(2 - h)),
             )
 
         def v_copy(layer, h, e):
             at = bit_of(h, e)
             return remote(
                 snd2.at[layer, 3, at, :], rec2.at[layer, 3, at, :],
-                v_send.at[layer, h, e], v_recv.at[layer, h, e], at_sp(peer(1 + h)),
+                r_send.at[layer], v_recv.at[layer, h, e], at_sp(peer(1 + h)),
             )
 
         def reduce_tile(layer, i):
             at = tile_at(flip(j, i))
             total = part[layer, c, at, :].astype(jnp.float32)
             for r in range(1, tp):
-                if timed:
-                    p_copy(layer, r, i).wait_recv()
-                else:
-                    p_copy(layer, r, i).wait()
+                p_copy(layer, r, i).wait_recv()
                 total = total + rec1[layer, r - 1, at, :].astype(jnp.float32)
             if i == 0:
                 acc[...] = total
@@ -612,7 +633,7 @@
 
         def relay(layer, h, e):
             if halves == 2:
-                v_copy(layer, h, e).wait()
+                v_copy(layer, h, e).wait_recv()
                 i, at = 2 - h, bit_of(h, e)
                 snd2[layer, i, at, :] = (
                     snd2[layer, i, at, :].astype(jnp.float32) + rec2[layer, 3, at, :].astype(jnp.float32)
@@ -696,14 +717,14 @@
             at = tile_at(flip(j, i))
             return remote(
                 part.at[last, lax.div(b, slots), at, cols_of(m)], rec1.at[last, 0, at, cols_of(m)],
-                p_send.at[last, m, i], p_recv.at[last, m, i], at_tp(1),
+                p_send.at[last, 0], p_recv.at[last, m, i], at_tp(1),
             )
 
         def b_copy(m, i, h):
             at = part_of(h)
             return remote(
                 snd2.at[last, i, at, cols_of(m)], rec2.at[last, i, at, cols_of(m)],
-                b_send.at[m, i, h], b_recv.at[m, i, h], at_sp(peer(i if i < 3 else 1 + h)),
+                b_send.at[0], b_recv.at[m, i - 1, h], at_sp(peer(i if i < 3 else 1 + h)),
             )
 
         def block_product(n):
@@ -755,23 +776,16 @@
                     if h == 0:
                         b_copy(m, 2, 1).start()
 
-        def block_sent():
-            for n in range(line):
-                b = nth_block(n)
-
-                @pl.when(lax.div(b, slots) != c)
-                def _():
-                    for i in range(q):
-                        q_copy(n, i).wait_send()
-
-            for m in range(slots):
-                for i in range(1, 4):
-                    for h in range(2):
-                        b_copy(m, i, h).wait_send()
+        def sums_sent(layer):
+            for r in range(1, tp):
+                take(part.at[layer, 0], p_send.at[layer, r - 1])
+                take(stat.at[layer], s_send.at[layer, r - 1])
+            if q > 1:
+                take(snd2.at[layer, pl.ds(0, q - 1)], b_send.at[0] if timed and layer == last else r_send.at[layer])
 
         def s_copy(layer, r, h):
             return remote(
-                stat.at[layer, h], stat_in.at[layer, r, h], s_send.at[layer, r, h], s_recv.at[layer, r, h], at_tp(r)
+                stat.at[layer, h], stat_in.at[layer, r, h], s_send.at[layer, r - 1], s_recv.at[layer, r - 1, h], at_tp(r)
             )
 
         def finish(layer, h):
@@ -783,9 +797,9 @@
                         b_copy(m, i, h).wait_recv()
                 elif halves == 2 and i == 2 - h:
                     for e in range(2):
-                        w_copy(layer, h, e).wait()
+                        w_copy(layer, h, e).wait_recv()
                 else:
-                    r_copy(layer, i, h).wait()
+                    r_copy(layer, i, h).wait_recv()
                 pre = pre + rec2[layer, i, at, :].astype(jnp.float32)
             acc[at, :] = pre
             own = jnp.sum(pre, axis=-1, keepdims=True)
@@ -797,7 +811,7 @@
                 s_copy(layer, r, h).start()
             sums, spreads = [own], [spread]
             for r in range(1, tp):
-                s_copy(layer, r, h).wait()
+                s_copy(layer, r, h).wait_recv()
                 sums.append(stat_in[layer, r, h, :, 0:1])
                 spreads.append(stat_in[layer, r, h, :, 1:2])
             mean = sum(sums[1:], sums[0]) * (1.0 / model)
@@ -821,7 +835,9 @@
 
         def first_half(layer, w0, w1, w2):
             def start():
-                gather_wait(layer, range(q))
+                gather_wait(layer, False)
+                if q > 3:
+                    gather_wait(layer, True)
                 arrived(layer * 4)
                 project(layer, layer, 0, put_u(0), ALL)
 
@@ -847,7 +863,7 @@
                 project(layer, layer, w, (put_u, put_z, put_o)[w](0), MOST)
 
         def rest_of(layer):
-            gather_wait(layer, (3,))
+            gather_wait(layer, True)
             project(layer, layer, 0, put_u(0), REST)
             project(layer, layer, 1, put_z(0), REST)
             halo_start(layer)
@@ -897,21 +913,21 @@
                 at_time(when, outward, k + 3, 1)
             for k, when in enumerate((54.2, 68.0, 79.0, 91.0)):
                 at_time(when, outward, k + 3, 2)
-            at_time(33.1, inner_wait, 0, (0, 1, 2))
+            at_time(33.1, inner_wait, 0, False)
             at_time(33.1, inner_arrived, 0)
             at_time(33.2, inner_project, 0, (0,), MOST)
             at_time(37.0, inner_arrived, 1)
             at_time(37.0, inner_project, 0, (1,), MOST)
-            at_time(43.5, inner_wait, far, (0, 1, 2))
+            at_time(43.5, inner_wait, far, False)
             at_time(43.6, inner_project, 1, (0, 1), MOST)
             at_time(45.5, inner_arrived, 2)
             at_time(45.6, inner_project, 1, (2,), MOST)
-            at_time(52.0, inner_wait, far, (3,))
+            at_time(52.0, inner_wait, far, True)
             at_time(52.1, inner_project, 1, (0, 1, 2), REST)
             at_time(53.1, far_gates)
             at_time(53.15, far_rest, 2, 1)
             at_time(53.18, inner_project, 0, (2,), MOST)
-            at_time(53.2, inner_wait, 0, (3,))
+            at_time(53.2, inner_wait, 0, True)
             at_time(53.21, inner_project, 0, (0, 1), REST)
             at_time(53.22, own_edge)
             at_time(53.23, far_first)
@@ -936,7 +952,7 @@
                 at_time(f + 0.1, gather_start, 1, h)
                 at_time(f + 9.0, gather_pass, 1, h)
                 at_time(93.0 + 0.1 * h, gather_last, 1, h)
-            at_time(88.0, gather_wait, 1, (0, 1, 2))
+            at_time(88.0, gather_wait, 1, False)
             at_time(88.1, most_of, 1, (0, 1))
             at_time(92.0, most_of, 1, (2,))
             at_time(94.0, rest_of, 1)
@@ -950,14 +966,13 @@
                 at_time(p, block_product, n)
                 at_time((126.0, 126.0, 126.5, 129.0)[n], block_relay, n)
             at_time(127.5, far_sent)
-            at_time(127.6, parts_sent)
             at_time(128.0, gather_sent, 1)
+            at_time(128.1, sums_sent, 0)
             for k in range(units):
-                for s in range(steps):
-                    at_time(129.5, line_sent, k, s)
+                at_time(129.5, all_sent, k)
             for h in range(halves):
                 at_time(130.0 + h, finish, last, h)
-            at_time(140.0, block_sent)
+            at_time(140.0, sums_sent, last)
         else:
             for k in range(units):
                 at_time(-2.0 if k < 2 else -1.0, scatter_start, k)
@@ -996,7 +1011,9 @@
         if not timed:
             for layer in range(layers):
                 gather_sent(layer)
+                sums_sent(layer)
             for k in range(units):
+                scatter_sent(k)
                 for s in range(steps):
                     line_sent(k, s)
 
@@ -1023,6 +1040,11 @@
         others = max(tp - 1, 1)
         banks = 2 if helped(line, q, tp, layers) else 1
         sets = layers + banks - 1
+        relays = 1 if banks == 2 else layers
+        if banks == 2:
+            lines = [dma((units,)), dma((units, steps)), dma((1,)), dma((1,))]
+        else:
+            lines = [dma((units, steps))] * 4
         halves = 2 if q == 4 else 1
         half_rows = rows // halves
         vm = pl.BlockSpec(memory_space=pltpu.VMEM)
@@ -1047,16 +1069,15 @@
                 pltpu.VMEM((layers, halves, half_rows, LANES), f32),
                 pltpu.VMEM((layers, tp, halves, half_rows, LANES), f32),
                 pltpu.VMEM((layers, 2, 8, width), f32),
-                dma((units, q)), dma((units, q)), dma((units,)),
-                dma((units, steps)), dma((units, steps)), dma((units, steps)), dma((units, steps)),
-                dma((sets, q, halves)), dma((sets, q, halves)), dma((halves,)),
-                dma((sets, tp, q, halves)), dma((sets, tp, q, halves)),
-                dma((layers, tp, q)), dma((layers, tp, q)),
-                dma((layers, q, 2)), dma((layers, q, 2)),
-                dma((layers, tp, halves)), dma((layers, tp, halves)),
+                dma((units,)), dma((units,)), *lines,
+                dma((sets,)), dma((sets, 3, halves)), dma((1,)),
+                dma((sets, others)), dma((sets, others, 2)),
+                dma((layers, others)), dma((layers, max(others, 2), q)),
+                dma((layers,)), dma((layers, 2)),
+                dma((layers, others)), dma((layers, others, halves)),
                 dma((layers,)), dma((layers,)),
-                dma((2, 4, 2)), dma((2, 4, 2)), dma((4,)), dma((4,)), dma((4,)), dma((4,)),
-                dma((layers, 2, 2)), dma((layers, 2, 2)), dma((layers, 2, 2)), dma((layers, 2, 2)),
+                dma((1,)), dma((2, 3, 2)), dma((1,)), dma((4,)), dma((1,)), dma((4,)),
+                dma((relays, 2, 2)), dma((relays, 2, 2)), dma((2,)),
             ],
             compiler_params=pltpu.CompilerParams(
                 collective_id=0, has_side_effects=True, vmem_limit_bytes=60 * 1024 * 1024

time: 147 us -> 144 us (0.980)
  Pallas kernels: 143 us -> 139 us
    pallas_call x1, Pallas kernels: 143 us -> 139 us  [shards(): pl.pallas_call(kernel, out_shape=jax.ShapeDtypeStruct((rows, feats), bf),...]
where the time goes in v4:
time: 144 us; the launch traced here: 141 us
  Pallas kernels  139 us (97%)
  local copies, waits for them, and re-layouts  1.87 us (1%)
    pallas_call x1, Pallas kernels, shards(): pl.pallas_call(kernel, out_shape=jax.ShapeDtypeStruct((rows, feats), bf),...  139 us

profile of v4, /device:TPU:25, one launch (start us, length us, event | category | flops | bytes accessed | tf_op | source)
XLA Modules:
  0.0 141.2 jit_solution(3990767164151441740)
XLA Ops:
  0.0 139.3 %shard_map.82 = bf16[256,1024]{1,0:T(8,128)(2,1)} custom-call(bf16[256,1024]{1,0:T(8,128)(2,1)} %tok.1, bf16[2,128,1024]{2,1,0:T(8,128)(2,1)} %val.1, bf16[2,128,1024]{2,1,0:T(8,128)(2,1)} %outw.1, bf16[2,128,1024]{2,1,0:T(8,128)(2,1)} %inn.1, f32[3,2,1024]{2,1,0:T(2,128)} %bitcast.1, bf16[2,1024,128]{2,1,0:T(8,128)(2,1)} %prj.1, f32[2,1024]{1,0:T(2,128)} %gain.1, ...), custom_call_target="tpu_custom_call" | custom-call | tf_op jit(solution)/shard_map/pallas_call | solution.py:1051
  139.3 1.9 %copy.10 = bf16[256,1024]{1,0:T(8,128)(2,1)} copy(bf16[256,1024]{1,0:T(8,128)(2,1)} %shard_map.82) | data formatting | bytes 1048576

commit v5 on v4

--- a/solution.py
+++ b/solution.py
@@ -434,9 +434,14 @@
                 at_sp(peer(1 + h)),
             )
 
-        def k_copy(i):
-            at = tile_at(flip(j, i))
-            return remote(gated.at[1, at, :], gated.at[0, at, :], k_send.at[0], k_recv.at[i], fellow())
+        def k_copy(tile):
+            at = tile_at(tile)
+            return remote(gated.at[1, at, :], gated.at[0, at, :], k_send.at[0], k_recv.at[tile], fellow())
+
+
+        odd = lax.rem(j, 2)
+        first_tile, second_tile = flip(j, 1), odd * j + (1 - odd) * flip(j, 2)
+        third_tile, fourth_tile = flip(j, 3), odd * flip(j, 2) + (1 - odd) * j
 
         def far_send():
             @outer
@@ -519,25 +524,45 @@
 
         tail = pl.ds(q * rows, 8)
 
+        def far_tiles(early):
+            for t in range(q):
+                soon = (t == first_tile) | (t == second_tile)
+
+                @pl.when(soon if early else jnp.logical_not(soon))
+                def _():
+                    convolve(0, 1, (t,))
+
+        def far_early():
+            @pl.when((l == 1) | ((l == 2) & (j == 0)))
+            def _():
+                zpad[1, 0:8, :] = jnp.zeros((8, width), jnp.float32)
+
+            @pl.when((l == 2) & (j > 0))
+            def _():
+                zpad[1, 0:8, :] = zpad[0, tail, :]
+
+            @inner
+            def _():
+                far_tiles(True)
+                k_copy(first_tile).start()
+                k_copy(second_tile).start()
+
         def far_gates():
-            @pl.when((l == 1) | ((l == 2) & (j == 0)))
-            def _():
-                zpad[1, 0:8, :] = jnp.zeros((8, width), jnp.float32)
-
-            @pl.when((l == 2) & (j > 0))
-            def _():
-                zpad[1, 0:8, :] = zpad[0, tail, :]
-
-            @inner
-            def _():
-                convolve(0, 1, range(q))
-                k_copy(q - 1).start()
+            @inner
+            def _():
+                far_tiles(False)
+                k_copy(third_tile).start()
+
+            @pl.when((l == 1) | ((l == 2) & (j > 0)))
+            def _():
+                k_copy(fourth_tile).start()
 
         def far_first():
             @pl.when((l == 2) & (j == 0))
             def _():
                 zpad[1, 0:8, :] = zpad[0, tail, :]
-                convolve(0, 1, range(1))
+                convolve(0, 1, (0,))
+                k_copy(fourth_tile).start()
 
         def own_gates():
             @lower_inner
@@ -552,12 +577,6 @@
             @inner
             def _():
                 convolve(0, 0, range(q))
-
-        def far_rest(*which):
-            @inner
-            def _():
-                for i in which:
-                    k_copy(i).start()
 
         def far_sent():
             @outer
@@ -665,32 +684,47 @@
         def late_half():
             return (l < line // 2).astype(jnp.int32)
 
-        def half_product(second):
+        def half_tile(second, i):
             cc = late_half() if second else 1 - late_half()
             weight = jnp.concatenate([wout[0, cc * per_half + b] for b in range(per_half)], axis=1)
-            for i in range(q - 1, -1, -1):
-                at = tile_at(flip(j, i))
-                if not second:
-                    @outer
-                    def _():
-                        k_copy(i).wait_recv()
-
-                part[0, cc, at, :] = jnp.dot(
-                    gated[0, at, :], weight, preferred_element_type=jnp.float32
-                ).astype(jnp.bfloat16)
-
-                @pl.when(cc != c)
+            at = tile_at(flip(j, i))
+            if not second:
+                @outer
                 def _():
-                    p_copy(0, 1, i).start()
-
-                if i < q - 1:
-                    @pl.when(cc == c)
-                    def _():
-                        reduce_tile(0, i + 1)
-
-            @pl.when(cc == c)
-            def _():
-                reduce_tile(0, 0)
+                    k_copy(flip(j, i)).wait_recv()
+
+            part[0, cc, at, :] = jnp.dot(
+                gated[0, at, :], weight, preferred_element_type=jnp.float32
+            ).astype(jnp.bfloat16)
+
+            @pl.when(cc != c)
+            def _():
+                p_copy(0, 1, i).start()
+
+        def half_sum(second, i):
+            @pl.when((late_half() == c) if second else (late_half() != c))
+            def _():
+                reduce_tile(0, i)
+
+        def inner_late_tile(i):
+            @inner
+            def _():
+                half_tile(True, i)
+
+        def inner_late_sum(i):
+            @inner
+            def _():
+                half_sum(True, i)
+
+        def outer_late_tile(i):
+            @outer
+            def _():
+                half_tile(True, i)
+
+        def outer_late_sum(i):
+            @outer
+            def _():
+                half_sum(True, i)
 
         def half_relay(second, h, e):
             @pl.when((late_half() == c) if second else (late_half() != c))
@@ -742,7 +776,11 @@
                 def _():
                     q_copy(n, i).start()
 
-            @pl.when(own)
+        def block_sum(n):
+            b = nth_block(n)
+            m = lax.rem(b, slots)
+
+            @pl.when(lax.div(b, slots) == c)
             def _():
                 for i in range(q - 1, -1, -1):
                     at = tile_at(flip(j, i))
@@ -887,7 +925,7 @@
 
         if timed:
             at_time(-1.0, far_send)
-            for when, k in ((0.0, 0), (0.1, 1), (0.2, 3), (0.3, 4), (0.5, 2), (0.6, 5), (13.7, 6), (13.8, 7)):
+            for when, k in ((0.0, 0), (0.1, 1), (0.2, 3), (0.3, 4), (0.5, 2), (0.6, 5), (0.7, 6), (0.8, 7)):
                 at_time(when, scatter_start, k)
             for h in range(halves):
                 at_time(0.4, inner_gather_start, h)
@@ -897,21 +935,21 @@
                 at_time(53.19 + 0.001 * h, inner_last, 0, h)
                 at_time(51.0 + 0.05 * h, inner_last, far, h)
             at_time(15.1, far_pass)
-            at_time(37.5, far_side)
+            at_time(43.1, far_side)
             at_time(42.5, far_diag)
             for k, when in enumerate((3.5, 6.5, 15.0, 15.2, 15.3, 18.0, 22.0, 24.0)):
                 at_time(when, outer_begin, k)
-            for k, when in enumerate((3.5, 6.5, 27.5, 9.5, 12.5, 30.0, 42.6, 42.7)):
+            for k, when in enumerate((3.5, 6.5, 27.5, 9.5, 12.5, 30.0, 38.0, 41.0)):
                 at_time(when, inner_ready, k)
-            for k, when in enumerate((3.6, 6.6, 27.6, 9.6, 54.22, 55.25, 66.0, 77.0)):
+            for k, when in enumerate((3.6, 6.6, 27.6, 9.6, 43.2, 57.1, 61.92, 66.2)):
                 at_time(when, inward, k, 0)
-            for k, when in enumerate((19.0, 25.0, 31.0, 51.5, 55.1, 60.0, 71.0, 83.0)):
+            for k, when in enumerate((19.0, 25.0, 31.0, 51.5, 57.0, 61.9, 66.1, 67.6)):
                 at_time(when, inward, k, 1)
-            for k, when in enumerate((9.7, 12.6, 30.1, 42.61, 42.71)):
+            for k, when in enumerate((9.7, 12.6, 30.1, 38.1, 41.1)):
                 at_time(when, outward, k + 3, 0)
-            for k, when in enumerate((23.5, 62.0, 73.0, 85.0, 97.0)):
+            for k, when in enumerate((23.5, 61.91, 67.5, 79.0, 87.1)):
                 at_time(when, outward, k + 3, 1)
-            for k, when in enumerate((54.2, 68.0, 79.0, 91.0)):
+            for k, when in enumerate((54.2, 66.0, 72.5, 82.0)):
                 at_time(when, outward, k + 3, 2)
             at_time(33.1, inner_wait, 0, False)
             at_time(33.1, inner_arrived, 0)
@@ -922,27 +960,32 @@
             at_time(43.6, inner_project, 1, (0, 1), MOST)
             at_time(45.5, inner_arrived, 2)
             at_time(45.6, inner_project, 1, (2,), MOST)
+            at_time(45.7, far_early)
             at_time(52.0, inner_wait, far, True)
             at_time(52.1, inner_project, 1, (0, 1, 2), REST)
             at_time(53.1, far_gates)
-            at_time(53.15, far_rest, 2, 1)
             at_time(53.18, inner_project, 0, (2,), MOST)
             at_time(53.2, inner_wait, 0, True)
             at_time(53.21, inner_project, 0, (0, 1), REST)
             at_time(53.22, own_edge)
             at_time(53.23, far_first)
-            at_time(53.24, far_rest, 0)
             at_time(54.21, inner_project, 0, (2,), REST)
             at_time(55.3, own_gates)
             o = 58.0
             at_time(o, line_end, 3, 0)
-            at_time(o, half_product, False)
+            for n, i in enumerate((1, 3, 2, 0)):
+                at_time(o + 0.1 * n, half_tile, False, i)
+                at_time(o + 0.1 * n + 0.15, half_sum, False, i)
             for e in range(2):
                 for h in range(2):
-                    at_time(o + 4.0 + 0.1 * e + 0.01 * h, half_relay, False, h, e)
-            at_time(o + 4.2, line_end, 3, 1)
-            at_time(o + 4.2, line_end, 3, 2)
-            at_time(o + 4.3, half_product, True)
+                    at_time(o + 8.5 + 0.1 * e + 0.01 * h, half_relay, False, h, e)
+            at_time(o + 8.75, line_end, 3, 1)
+            at_time(o + 8.75, line_end, 3, 2)
+            for n, i in enumerate((3, 2, 1, 0)):
+                at_time(o + 4.3 + 0.1 * n, inner_late_tile, i)
+                at_time(o + 4.3 + 0.1 * n + 0.15, inner_late_sum, i)
+                at_time(o + 8.8 + 0.01 * n, outer_late_tile, i)
+                at_time(o + 8.8 + 0.01 * n + 0.015, outer_late_sum, i)
             for e in range(2):
                 for h in range(2):
                     at_time(o + 9.0 + 0.1 * e + 0.01 * h, half_relay, True, h, e)
@@ -954,17 +997,17 @@
                 at_time(93.0 + 0.1 * h, gather_last, 1, h)
             at_time(88.0, gather_wait, 1, False)
             at_time(88.1, most_of, 1, (0, 1))
-            at_time(92.0, most_of, 1, (2,))
-            at_time(94.0, rest_of, 1)
-            at_time(103.0, outward, units - 1, 2)
-            at_time(106.2, gates_of, 1)
+            at_time(93.2, rest_of, 1)
+            at_time(93.4, most_of, 1, (2,))
+            at_time(93.5, outward, units - 1, 2)
+            at_time(94.0, gates_of, 1)
             at_time(128.0, halo_sent, 1)
+            for n in range(1, line):
+                at_time((110.0, 110.1, 111.0, 113.0)[n], line_end, units - 1, n - 1)
             for n in range(line):
-                p = (110.0, 114.0, 119.0, 125.0)[n]
-                if n:
-                    at_time(p, line_end, 7, n - 1)
-                at_time(p, block_product, n)
-                at_time((126.0, 126.0, 126.5, 129.0)[n], block_relay, n)
+                at_time((110.0, 110.2, 111.0, 113.0)[n], block_product, n)
+                at_time((110.3, 110.4, 111.1, 113.5)[n], block_sum, n)
+                at_time((113.1, 113.2, 114.0, 114.1)[n], block_relay, n)
             at_time(127.5, far_sent)
             at_time(128.0, gather_sent, 1)
             at_time(128.1, sums_sent, 0)

time: 144 us -> 141 us (0.979)
  Pallas kernels: 139 us -> 137 us
    pallas_call x1, Pallas kernels: 139 us -> 137 us  [shards(): pl.pallas_call(kernel, out_shape=jax.ShapeDtypeStruct((rows, feats), bf),...]
where the time goes in v5:
time: 141 us; the launch traced here: 139 us
  Pallas kernels  137 us (97%)
  local copies, waits for them, and re-layouts  1.87 us (1%)
    pallas_call x1, Pallas kernels, shards(): pl.pallas_call(kernel, out_shape=jax.ShapeDtypeStruct((rows, feats), bf),...  137 us

profile of v5, /device:TPU:25, one launch (start us, length us, event | category | flops | bytes accessed | tf_op | source)
XLA Modules:
  0.0 139.2 jit_solution(16468185625893824878)
XLA Ops:
  0.0 137.3 %shard_map.82 = bf16[256,1024]{1,0:T(8,128)(2,1)} custom-call(bf16[256,1024]{1,0:T(8,128)(2,1)} %tok.1, bf16[2,128,1024]{2,1,0:T(8,128)(2,1)} %val.1, bf16[2,128,1024]{2,1,0:T(8,128)(2,1)} %outw.1, bf16[2,128,1024]{2,1,0:T(8,128)(2,1)} %inn.1, f32[3,2,1024]{2,1,0:T(2,128)} %bitcast.1, bf16[2,1024,128]{2,1,0:T(8,128)(2,1)} %prj.1, f32[2,1024]{1,0:T(2,128)} %gain.1, ...), custom_call_target="tpu_custom_call" | custom-call | tf_op jit(solution)/shard_map/pallas_call | solution.py:1094
  137.3 1.9 %copy.10 = bf16[256,1024]{1,0:T(8,128)(2,1)} copy(bf16[256,1024]{1,0:T(8,128)(2,1)} %shard_map.82) | data formatting | bytes 1048576

commit v6 on v5

--- a/solution.py
+++ b/solution.py
@@ -41,12 +41,12 @@
     block_cols = q * out_cols
 
     def kernel(
-        tok, val, outw, inn, taps, prj, gain, bias, res,
+        tok_in, val_in, outw_in, inn_in, taps, prj_in, gain, bias, res,
         xg, win, wout, ubuf, obuf, zpad, gated, part, rec1, snd2, rec2, acc, stat, stat_in, halo,
         a_send, a_recv, u_send, u_recv, d_send, d_recv,
         g_send, g_recv, g_loc, t_send, t_recv, p_send, p_recv, r_send, r_recv, s_send, s_recv, h_send, h_recv,
         b_send, b_recv, n_send, n_recv, k_send, k_recv,
-        v_recv, w_recv, e_recv,
+        v_recv, w_recv, e_recv, tok, val, outw, inn, prj, in_sem,
     ):
         me = lax.axis_index("sp")
         c = lax.axis_index("tp")
@@ -68,6 +68,15 @@
         def peer(i):
             return l * q + flip(j, i)
 
+        loads = [
+            pltpu.make_async_copy(src, dst, in_sem.at[n])
+            for n, (src, dst) in enumerate(
+                ((tok_in, tok), (val_in, val), (inn_in, inn), (prj_in, prj), (outw_in, outw))
+            )
+        ]
+        for load in loads:
+            load.start()
+
         barrier = pltpu.get_barrier_semaphore()
 
         def greet(dev):
@@ -88,6 +97,8 @@
 
         neighbours = (l > 0).astype(jnp.int32) + (l < line - 1).astype(jnp.int32)
         pl.semaphore_wait(barrier, (q - 1) + (tp - 1) + neighbours)
+        for load in loads:
+            load.wait()
 
 
         ORDER = (val, inn, outw, prj)
@@ -290,10 +301,13 @@
         def rows_like(n):
             return xg.at[0, 0, pl.ds(0, n * rows), :]
 
+        def kind(layer, i):
+            return 1 if i == 3 else 2 if i == 0 and timed and layer else 0
+
         def t_copy(layer, r, i, h):
             src = mine(layer, h) if i == 0 else spot(layer, flip(j, i), h)
             return remote(
-                src, spot(layer, flip(j, i), h), t_send.at[layer, r - 1], t_recv.at[layer, r - 1, i // 3], at_tp(r)
+                src, spot(layer, flip(j, i), h), t_send.at[layer, r - 1], t_recv.at[layer, r - 1, kind(layer, i)], at_tp(r)
             )
 
         def cross_start(layer, i, h):
@@ -332,9 +346,14 @@
 
         def gather_wait(layer, rest):
             for r in range(1, tp):
-                take(rows_like(1 if rest else min(q, 3)), t_recv.at[layer, r - 1, 1 if rest else 0])
+                n = 1 if rest else 2 if timed and layer else min(q, 3)
+                take(rows_like(n), t_recv.at[layer, r - 1, 1 if rest else 0])
             if layer == 0 and not rest:
                 take(rows_like(1), g_loc.at[0])
+
+        def gather_own(layer):
+            for r in range(1, tp):
+                take(rows_like(1), t_recv.at[layer, r - 1, 2])
 
         def gather_sent(layer):
             if q > 1:
@@ -347,13 +366,18 @@
 
 
         far = layers
-        ALL, MOST, REST = (0, q), (1, q - 1), (0, 1)
+        ALL, MOST, REST, OWN, SIDE = (0, q), (1, q - 1), (0, 1), (0, 1, 0), (0, 2, 0)
 
         def project(rows_set, layer, w, store, span):
             first = flip(j, q - 1) if span is not ALL else 0
 
             def tile(n, carry):
-                i = lax.rem(first + span[0] + n, q)
+                if span is OWN:
+                    i = j
+                elif span is SIDE:
+                    i = flip(j, 1) + n * (flip(j, 2) - flip(j, 1))
+                else:
+                    i = lax.rem(first + span[0] + n, q)
                 at = tile_at(i)
                 total = jnp.zeros((rows, width), jnp.float32)
                 for cc in range(tp):
@@ -510,6 +534,11 @@
             def _():
                 for w in ws:
                     project(far if bank else 0, 0, w, (put_u, put_z, put_o)[w](bank), span)
+
+        def inner_own():
+            @inner
+            def _():
+                gather_own(far)
 
         def inner_arrived(k):
             @inner
@@ -895,10 +924,10 @@
             at_time(w1, middle)
             at_time(w2, gates)
 
-        def most_of(layer, ws):
-            for w in ws:
+        def some_of(layer, w, span, fresh):
+            if fresh:
                 arrived(layer * 4 + w)
-                project(layer, layer, w, (put_u, put_z, put_o)[w](0), MOST)
+            project(layer, layer, w, (put_u, put_z, put_o)[w](0), span)
 
         def rest_of(layer):
             gather_wait(layer, True)
@@ -957,7 +986,9 @@
             at_time(37.0, inner_arrived, 1)
             at_time(37.0, inner_project, 0, (1,), MOST)
             at_time(43.5, inner_wait, far, False)
-            at_time(43.6, inner_project, 1, (0, 1), MOST)
+            at_time(38.2, inner_own)
+            at_time(38.2, inner_project, 1, (0, 1), OWN)
+            at_time(43.6, inner_project, 1, (0, 1), SIDE)
             at_time(45.5, inner_arrived, 2)
             at_time(45.6, inner_project, 1, (2,), MOST)
             at_time(45.7, far_early)
@@ -996,9 +1027,13 @@
                 at_time(f + 9.0, gather_pass, 1, h)
                 at_time(93.0 + 0.1 * h, gather_last, 1, h)
             at_time(88.0, gather_wait, 1, False)
-            at_time(88.1, most_of, 1, (0, 1))
+            at_time(82.5, gather_own, 1)
+            at_time(82.5, some_of, 1, 0, OWN, True)
+            at_time(87.2, some_of, 1, 1, OWN, True)
+            at_time(88.1, some_of, 1, 0, SIDE, False)
+            at_time(88.1, some_of, 1, 1, SIDE, False)
+            at_time(93.15, some_of, 1, 2, MOST, True)
             at_time(93.2, rest_of, 1)
-            at_time(93.4, most_of, 1, (2,))
             at_time(93.5, outward, units - 1, 2)
             at_time(94.0, gates_of, 1)
             at_time(128.0, halo_sent, 1)
@@ -1090,11 +1125,11 @@
             lines = [dma((units, steps))] * 4
         halves = 2 if q == 4 else 1
         half_rows = rows // halves
-        vm = pl.BlockSpec(memory_space=pltpu.VMEM)
+        vm, hbm = pl.BlockSpec(memory_space=pltpu.VMEM), pl.BlockSpec(memory_space=pl.ANY)
         return pl.pallas_call(
             kernel,
             out_shape=jax.ShapeDtypeStruct((rows, feats), bf),
-            in_specs=[vm] * 8,
+            in_specs=[hbm] * 4 + [vm, hbm, vm, vm],
             out_specs=vm,
             scratch_shapes=[
                 pltpu.VMEM((layers + banks - 1, tp, q * rows, feats), bf),
@@ -1114,13 +1149,15 @@
                 pltpu.VMEM((layers, 2, 8, width), f32),
                 dma((units,)), dma((units,)), *lines,
                 dma((sets,)), dma((sets, 3, halves)), dma((1,)),
-                dma((sets, others)), dma((sets, others, 2)),
+                dma((sets, others)), dma((sets, others, 3)),
                 dma((layers, others)), dma((layers, max(others, 2), q)),
                 dma((layers,)), dma((layers, 2)),
                 dma((layers, others)), dma((layers, others, halves)),
                 dma((layers,)), dma((layers,)),
                 dma((1,)), dma((2, 3, 2)), dma((1,)), dma((4,)), dma((1,)), dma((4,)),
                 dma((relays, 2, 2)), dma((relays, 2, 2)), dma((2,)),
+                *[pltpu.VMEM(a.shape, bf) for a in (tokens, value_weight, outer_weight, inner_weight, output_weight)],
+                dma((5,)),
             ],
             compiler_params=pltpu.CompilerParams(
                 collective_id=0, has_side_effects=True, vmem_limit_bytes=60 * 1024 * 1024

time: 141 us -> 139 us (0.986); the launches traced: 139 us -> 139 us
  no operation moved by 1% of the time
where the time goes in v6:
time: 139 us
  Pallas kernels  137 us (99%)
  local copies, waits for them, and re-layouts  1.87 us (1%)
    pallas_call x1, Pallas kernels, shards(): pl.pallas_call(kernel, out_shape=jax.ShapeDtypeStruct((rows, feats), bf),...  137 us

profile of v6, /device:TPU:25, one launch (start us, length us, event | category | flops | bytes accessed | tf_op | source)
XLA Modules:
  0.0 138.7 jit_solution(9510989443370679942)
XLA Ops:
  0.0 136.8 %shard_map.82 = bf16[256,1024]{1,0:T(8,128)(2,1)} custom-call(bf16[256,1024]{1,0:T(8,128)(2,1)} %tok_in.1, bf16[2,128,1024]{2,1,0:T(8,128)(2,1)} %val_in.1, bf16[2,128,1024]{2,1,0:T(8,128)(2,1)} %outw_in.1, bf16[2,128,1024]{2,1,0:T(8,128)(2,1)} %inn_in.1, f32[3,2,1024]{2,1,0:T(2,128)} %bitcast.1, bf16[2,1024,128]{2,1,0:T(8,128)(2,1)} %prj_in.1, ...), custom_call_target="tpu_custom_call" | custom-call | tf_op jit(solution)/shard_map/pallas_call | solution.py:1129
  136.8 1.9 %copy.10 = bf16[256,1024]{1,0:T(8,128)(2,1)} copy(bf16[256,1024]{1,0:T(8,128)(2,1)} %shard_map.82) | data formatting | bytes 1048576

commit v7 on v6

--- a/solution.py
+++ b/solution.py
@@ -269,6 +269,13 @@
             @inner
             def _():
                 take(xg.at[0, 0, pl.ds(0, (2 if k < 3 else 5) * each), :], u_send.at[k])
+
+        def outward_for(held, k, s):
+            holder = (l == 1) & (c == 1)
+
+            @pl.when(holder if held else jnp.logical_not(holder))
+            def _():
+                outward(k, s)
 
 
         def part_of(h):
@@ -976,10 +983,13 @@
                 at_time(when, inward, k, 1)
             for k, when in enumerate((9.7, 12.6, 30.1, 38.1, 41.1)):
                 at_time(when, outward, k + 3, 0)
-            for k, when in enumerate((23.5, 61.91, 67.5, 79.0, 87.1)):
-                at_time(when, outward, k + 3, 1)
-            for k, when in enumerate((54.2, 66.0, 72.5, 82.0)):
-                at_time(when, outward, k + 3, 2)
+            for k, when in ((3, 23.5), (5, 67.5), (6, 79.0), (7, 87.1)):
+                at_time(when, outward, k, 1)
+            for k, when in ((3, 54.2), (5, 72.5), (6, 82.0)):
+                at_time(when, outward, k, 2)
+            for s in range(1, 3):
+                at_time((61.91, 66.0)[s - 1], outward_for, False, 4, s)
+                at_time(67.0005 + 0.0001 * s, outward_for, True, 4, s)
             at_time(33.1, inner_wait, 0, False)
             at_time(33.1, inner_arrived, 0)
             at_time(33.2, inner_project, 0, (0,), MOST)

time: 139 us -> 139 us (level)
  no operation moved by 1% of the time
where the time goes in v7:
time: 139 us
  Pallas kernels  137 us (99%)
  local copies, waits for them, and re-layouts  1.87 us (1%)
    pallas_call x1, Pallas kernels, shards(): pl.pallas_call(kernel, out_shape=jax.ShapeDtypeStruct((rows, feats), bf),...  137 us

profile of v7, /device:TPU:25, one launch (start us, length us, event | category | flops | bytes accessed | tf_op | source)
XLA Modules:
  0.0 138.7 jit_solution(13280739756342492713)
XLA Ops:
  0.0 136.8 %shard_map.82 = bf16[256,1024]{1,0:T(8,128)(2,1)} custom-call(bf16[256,1024]{1,0:T(8,128)(2,1)} %tok_in.1, bf16[2,128,1024]{2,1,0:T(8,128)(2,1)} %val_in.1, bf16[2,128,1024]{2,1,0:T(8,128)(2,1)} %outw_in.1, bf16[2,128,1024]{2,1,0:T(8,128)(2,1)} %inn_in.1, f32[3,2,1024]{2,1,0:T(2,128)} %bitcast.1, bf16[2,1024,128]{2,1,0:T(8,128)(2,1)} %prj_in.1, ...), custom_call_target="tpu_custom_call" | custom-call | tf_op jit(solution)/shard_map/pallas_call | solution.py:1139
  136.8 1.9 %copy.10 = bf16[256,1024]{1,0:T(8,128)(2,1)} copy(bf16[256,1024]{1,0:T(8,128)(2,1)} %shard_map.82) | data formatting | bytes 1048576
